TPU v7x, 32 devices: a whole 2x2x4 slice. The times are simulated.
32 devices in a mesh: tp: 4 (over y, x), dp: 8 (over z, core).
Axes of the slice: x: 2, y: 2, z: 4, core: 2. Of those that a mesh axis runs over, the one named last changes fastest.
Arguments:
- tokens: bfloat16 [16, 4096], P('tp', 'dp'), may hold values from -12.5 to 12.5
- gain_first: bfloat16 [4096], P('dp'), may hold values from 0.099609375 to 1.8984375
- query_first: bfloat16 [4096, 2048], P('dp', 'tp'), may hold values from -0.09375 to 0.09375
- key_first: bfloat16 [4096, 2048], P('dp', 'tp'), may hold values from -0.09375 to 0.09375
- value_first: bfloat16 [4096, 4096], P('dp', 'tp'), may hold values from -0.09375 to 0.09375
- outgate_first: bfloat16 [4096, 4096], P('dp', 'tp'), may hold values from -0.09375 to 0.09375
- inputgate_first: bfloat16 [4096, 16], P('dp'), may hold values from -0.09375 to 0.09375
- forget_first: bfloat16 [4096, 16], P('dp'), may hold values from -0.09375 to 0.09375
- mixing_first: bfloat16 [4096, 4096], P('tp', 'dp'), may hold values from -0.09375 to 0.09375
- cell_first: float32 [16, 16, 256, 128], P('dp', 'tp'), may hold values from -6 to 6
- norm_first: float32 [16, 16, 128], P('dp', 'tp'), may hold values from -6 to 6
- stabilizer_first: float32 [16, 16], P('dp', 'tp'), may hold values from -3 to 115
- gain_second: bfloat16 [4096], P('dp'), may hold values from 0.099609375 to 1.8984375
- query_second: bfloat16 [4096, 2048], P('dp', 'tp'), may hold values from -0.09375 to 0.09375
- key_second: bfloat16 [4096, 2048], P('dp', 'tp'), may hold values from -0.09375 to 0.09375
- value_second: bfloat16 [4096, 4096], P('dp', 'tp'), may hold values from -0.09375 to 0.09375
- outgate_second: bfloat16 [4096, 4096], P('dp', 'tp'), may hold values from -0.09375 to 0.09375
- inputgate_second: bfloat16 [4096, 16], P('dp'), may hold values from -0.09375 to 0.09375
- forget_second: bfloat16 [4096, 16], P('dp'), may hold values from -0.09375 to 0.09375
- mixing_second: bfloat16 [4096, 4096], P('tp', 'dp'), may hold values from -0.09375 to 0.09375
- cell_second: float32 [16, 16, 256, 128], P('dp', 'tp'), may hold values from -6 to 6
- norm_second: float32 [16, 16, 128], P('dp', 'tp'), may hold values from -6 to 6
- stabilizer_second: float32 [16, 16], P('dp', 'tp'), may hold values from -3 to 115
Outputs:
- hidden: bfloat16 [16, 4096], P('tp', 'dp')
- cell_first_next: float32 [16, 16, 256, 128], P('dp', 'tp')
- norm_first_next: float32 [16, 16, 128], P('dp', 'tp')
- stabilizer_first_next: float32 [16, 16], P('dp', 'tp')
- cell_second_next: float32 [16, 16, 256, 128], P('dp', 'tp')
- norm_second_next: float32 [16, 16, 128], P('dp', 'tp')
- stabilizer_second_next: float32 [16, 16], P('dp', 'tp')
All inputs are finite; a program needn't handle non-finite values.
Results may differ from a plain program's by a relative error of at most 0.023.
Values may be sent and summed in bfloat16 or wider, within the bound.
No kernel may reach another device: no remote copies, remote signals or barrier semaphores. Data moves between devices by JAX's collectives and lax.ppermute only.
A program may use at most 64 MiB of HBM per device.

v0:
```python
import jax
import jax.numpy as jnp
from jax import lax
from jax.sharding import PartitionSpec as P

D = 4096
DHK = 128
DHV = 256


eps = 1e-06


def cell_step(
    x_shard,
    gain,
    w_query,
    w_key,
    w_value,
    w_outgate,
    w_input,
    w_forget,
    w_mixing,
    cell_state,
    norm_state,
    stabilizer,
):
    seq_count = cell_state.shape[0]
    local_heads = cell_state.shape[1]
    gathered = lax.all_gather(x_shard, "tp", axis=0, tiled=True)
    widened = gathered.astype(jnp.float32)
    squares = jnp.sum(widened * widened, axis=1)
    scaled = (widened * gain.astype(jnp.float32)).astype(jnp.bfloat16)

    def project(weight):
        return jnp.dot(scaled, weight, preferred_element_type=jnp.float32)

    query_part, key_part, input_part, forget_part, own_squares = (
        lax.psum_scatter(project(w_query), "dp", scatter_dimension=0, tiled=True),
        lax.psum_scatter(project(w_key), "dp", scatter_dimension=0, tiled=True),
        lax.psum_scatter(project(w_input), "dp", scatter_dimension=0, tiled=True),
        lax.psum_scatter(project(w_forget), "dp", scatter_dimension=0, tiled=True),
        lax.psum_scatter(squares, "dp", scatter_dimension=0, tiled=True),
    )
    row_scale = lax.rsqrt(own_squares / D + eps)[:, None]
    offset = lax.axis_index("tp") * local_heads
    input_pre = lax.dynamic_slice_in_dim(input_part * row_scale, offset, local_heads, 1)
    forget_pre = lax.dynamic_slice_in_dim(forget_part * row_scale, offset, local_heads, 1)
    queries = (query_part * row_scale).reshape(seq_count, local_heads, DHK) * DHK ** (-0.5)
    key_rows = (key_part * row_scale).reshape(seq_count, local_heads, DHK)
    log_forget = jax.nn.log_sigmoid(forget_pre)
    stab_next = jnp.maximum(log_forget + stabilizer, input_pre)
    retain = jnp.exp(log_forget + stabilizer - stab_next)
    admitted = jnp.exp(input_pre - stab_next)
    kept_cell = retain[:, :, None, None] * cell_state
    kept_norm = retain[:, :, None] * norm_state
    value_part, outgate_part = (
        lax.psum_scatter(
            project(w_value).astype(jnp.bfloat16), "dp", scatter_dimension=0, tiled=True
        ).astype(jnp.float32),
        lax.psum_scatter(
            project(w_outgate).astype(jnp.bfloat16), "dp", scatter_dimension=0, tiled=True
        ).astype(jnp.float32),
    )
    value_rows = (value_part * row_scale).reshape(seq_count, local_heads, DHV)
    cell_next = (
        kept_cell + admitted[:, :, None, None] * value_rows[:, :, :, None] * key_rows[:, :, None, :]
    )
    norm_next = kept_norm + admitted[:, :, None] * key_rows
    numerator = jnp.einsum("shvd,shd->shv", cell_next, queries, precision=lax.Precision.HIGHEST)
    denominator = jnp.einsum("shd,shd->sh", norm_next, queries, precision=lax.Precision.HIGHEST)
    readout = numerator / jnp.maximum(jnp.abs(denominator), 1.0)[:, :, None]
    gated_rows = (
        readout.reshape(seq_count, local_heads * DHV) * jax.nn.sigmoid(outgate_part * row_scale)
    ).astype(jnp.bfloat16)
    partial_value = jnp.dot(
        lax.all_gather(gated_rows, "dp", axis=0, tiled=True),
        w_mixing,
        preferred_element_type=jnp.float32,
    )
    summed = lax.psum_scatter(
        partial_value.astype(jnp.bfloat16), "tp", scatter_dimension=0, tiled=True
    ).astype(jnp.float32)
    result = (x_shard.astype(jnp.float32) + summed).astype(jnp.bfloat16)
    return (result, cell_next, norm_next, stab_next)


def per_device(
    tokens,
    gain_first,
    query_first,
    key_first,
    value_first,
    outgate_first,
    inputgate_first,
    forget_first,
    mixing_first,
    cell_first,
    norm_first,
    stabilizer_first,
    gain_second,
    query_second,
    key_second,
    value_second,
    outgate_second,
    inputgate_second,
    forget_second,
    mixing_second,
    cell_second,
    norm_second,
    stabilizer_second,
):
    middle, cell_one, norm_one, stab_one = cell_step(
        tokens,
        gain_first,
        query_first,
        key_first,
        value_first,
        outgate_first,
        inputgate_first,
        forget_first,
        mixing_first,
        cell_first,
        norm_first,
        stabilizer_first,
    )
    hidden, cell_two, norm_two, stab_two = cell_step(
        middle,
        gain_second,
        query_second,
        key_second,
        value_second,
        outgate_second,
        inputgate_second,
        forget_second,
        mixing_second,
        cell_second,
        norm_second,
        stabilizer_second,
    )
    return (hidden, cell_one, norm_one, stab_one, cell_two, norm_two, stab_two)


def solution(mesh):
    return jax.shard_map(
        per_device,
        mesh=mesh,
        in_specs=(
            P("tp", "dp"),
            P("dp"),
            P("dp", "tp"),
            P("dp", "tp"),
            P("dp", "tp"),
            P("dp", "tp"),
            P("dp", None),
            P("dp", None),
            P("tp", "dp"),
            P("dp", "tp", None, None),
            P("dp", "tp", None),
            P("dp", "tp"),
            P("dp"),
            P("dp", "tp"),
            P("dp", "tp"),
            P("dp", "tp"),
            P("dp", "tp"),
            P("dp", None),
            P("dp", None),
            P("tp", "dp"),
            P("dp", "tp", None, None),
            P("dp", "tp", None),
            P("dp", "tp"),
        ),
        out_specs=(
            P("tp", "dp"),
            P("dp", "tp", None, None),
            P("dp", "tp", None),
            P("dp", "tp"),
            P("dp", "tp", None, None),
            P("dp", "tp", None),
            P("dp", "tp"),
        ),
        check_vma=False,
    )
```

profile of v0, /device:TPU:0, one launch (start us, length us, event | category | flops | bytes accessed | tf_op | source)
XLA Modules:
  0.0 333.4 jit_solution(16564015335586895020)
XLA Ops:
  7.2 0.8 convert_element_type.74
  8.0 9.7 %all-gather = bf16[4,4,512]{2,1,0:T(4,128)(2,1)S(1)} all-gather(bf16[1,4,512]{2,1,0:T(4,128)(2,1)S(1)} %bitcast.57), channel_id=1, replica_groups=mesh['tp'=4,'dp'=8] {'tp'}, dimensions={0}, use_global_device_ids=true | all-gather | bytes 20480 | tf_op jit(solution)/shard_map/all_gather | solution.py:30
  17.7 0.6 multiply_reduce_fusion.1
  18.3 1.4 fusion.26
  19.8 1.4 fusion.25
  21.2 1.9 fusion.28
  23.1 0.8 fusion.27
  24.0 0.9 convolution_convert_fusion.2
  24.9 0.9 convolution_convert_fusion.3
  25.9 0.6 copy-done.25
  26.5 0.6 dynamic-slice.14
  27.2 0.6 dynamic-slice
  29.1 46.7 %all-reduce.27.cloned.1.call-done = (f32[16,512]{1,0:T(8,128)}, f32[16]{0:T(128)}, f32[16,16]{1,0:T(8,128)}, f32[16,16]{1,0:T(8,128)}, f32[16,512]{1,0:T(8,128)}) async-done(((f32[16,512]{1,0:T(8,128)}, f32[16]{0:T(128)}, f32[16,16]{1,0:T(8,128)}, f32[16,16]{1,0:T(8,128)}, f32[16,512]{1,0:T(8,128)}), (f32[16,512]{1,0:T(8,128)}, f32[16]{0:T(128)}, f32[16,16]{1,0:T(8,128)}, f32[16,16]{1,0:T(8,128)}, ...) | async-done | bytes 67664
  75.9 0.6 copy-done.22
  76.6 0.8 fusion.5
  77.4 0.7 fusion.9
  78.1 0.7 copy-done.20
  79.0 0.5 copy-done.17
  79.5 0.7 copy-done.15
  80.2 0.7 multiply_reduce_fusion.3
  80.9 55.4 %all-reduce.31.cloned.1.call-done = (bf16[16,1024]{1,0:T(8,128)(2,1)}, bf16[16,1024]{1,0:T(8,128)(2,1)}) async-done(((bf16[16,1024]{1,0:T(8,128)(2,1)}, bf16[16,1024]{1,0:T(8,128)(2,1)}), (bf16[16,1024]{1,0:T(8,128)(2,1)}, bf16[16,1024]{1,0:T(8,128)(2,1)})) %all-reduce.31.cloned.1.call-update) | async-done | bytes 65552
  136.2 0.8 convert_multiply_fusion.1
  137.5 1.0 fusion.29
  138.6 0.8 fusion.7
  139.4 14.1 %all-gather.1 = bf16[8,2,1024]{2,1,0:T(2,128)(2,1)S(1)} all-gather(bf16[1,2,1024]{2,1,0:T(2,128)(2,1)S(1)} %fusion.7), channel_id=1, replica_groups=mesh['tp'=4,'dp'=8] {'dp'}, dimensions={0}, use_global_device_ids=true | all-gather | bytes 36864 | tf_op jit(solution)/shard_map/all_gather | solution.py:77
  153.8 16.0 %all-reduce.7 = bf16[16,512]{1,0:T(8,128)(2,1)S(1)} all-reduce(bf16[16,512]{1,0:T(8,128)(2,1)S(1)} %convolution_convert_fusion.5), channel_id=9, replica_groups=mesh['tp'=4,'dp'=8] {'tp'}, use_global_device_ids=true, to_apply=%region_8.9.clone | all-reduce | flops 8192 | bytes 32768
  169.7 7.2 %all-gather.2 = bf16[4,4,512]{2,1,0:T(4,128)(2,1)S(1)} all-gather(bf16[1,4,512]{2,1,0:T(4,128)(2,1)S(1)} %fusion.22), channel_id=1, replica_groups=mesh['tp'=4,'dp'=8] {'tp'}, dimensions={0}, use_global_device_ids=true | all-gather | bytes 20480 | tf_op jit(solution)/shard_map/all_gather | solution.py:30
  177.0 0.6 multiply_reduce_fusion
  177.7 0.7 fusion.31
  178.4 0.7 fusion.30
  179.2 2.2 convolution_convert_fusion
  181.3 0.8 fusion.33
  182.1 0.8 fusion.32
  183.0 0.9 convolution_convert_fusion.1
  183.9 48.7 %all-reduce.25.cloned.1.call-done = (f32[16,512]{1,0:T(8,128)}, f32[16]{0:T(128)}, f32[16,16]{1,0:T(8,128)}, f32[16,16]{1,0:T(8,128)}, f32[16,512]{1,0:T(8,128)}) async-done(((f32[16,512]{1,0:T(8,128)}, f32[16]{0:T(128)}, f32[16,16]{1,0:T(8,128)}, f32[16,16]{1,0:T(8,128)}, f32[16,512]{1,0:T(8,128)}), (f32[16,512]{1,0:T(8,128)}, f32[16]{0:T(128)}, f32[16,16]{1,0:T(8,128)}, f32[16,16]{1,0:T(8,128)}, ...) | async-done | bytes 67664
  232.6 0.6 copy-done.23
  233.3 0.8 fusion.4
  234.1 0.8 fusion.11
  234.9 0.7 copy-done.21
  236.2 0.7 copy-done.16
  236.9 0.7 multiply_reduce_fusion.2
  237.6 55.2 %all-reduce.29.cloned.1.call-done = (bf16[16,1024]{1,0:T(8,128)(2,1)}, bf16[16,1024]{1,0:T(8,128)(2,1)}) async-done(((bf16[16,1024]{1,0:T(8,128)(2,1)}, bf16[16,1024]{1,0:T(8,128)(2,1)}), (bf16[16,1024]{1,0:T(8,128)(2,1)}, bf16[16,1024]{1,0:T(8,128)(2,1)})) %all-reduce.29.cloned.1.call-update) | async-done | bytes 65552
  292.8 0.8 convert_multiply_fusion
  294.1 1.0 fusion.34
  295.1 0.8 fusion.6
  296.0 14.1 %all-gather.3 = bf16[8,2,1024]{2,1,0:T(2,128)(2,1)S(1)} all-gather(bf16[1,2,1024]{2,1,0:T(2,128)(2,1)S(1)} %fusion.6), channel_id=1, replica_groups=mesh['tp'=4,'dp'=8] {'dp'}, dimensions={0}, use_global_device_ids=true | all-gather | bytes 36864 | tf_op jit(solution)/shard_map/all_gather | solution.py:77
  310.3 16.0 %all-reduce.15 = bf16[16,512]{1,0:T(8,128)(2,1)S(1)} all-reduce(bf16[16,512]{1,0:T(8,128)(2,1)S(1)} %convolution_convert_fusion.4), channel_id=17, replica_groups=mesh['tp'=4,'dp'=8] {'tp'}, use_global_device_ids=true, to_apply=%region_17.18.clone | all-reduce | flops 8192 | bytes 32768
  326.3 0.6 add_convert_fusion
  (84 shorter events, 3.3 us)
Async XLA Ops:
  7.2 16.8 %copy-start = (bf16[512,1024]{1,0:T(8,128)(2,1)S(1)}, bf16[512,1024]{1,0:T(8,128)(2,1)}, u32[]{:S(2)}) copy-start(bf16[512,1024]{1,0:T(8,128)(2,1)} %param.28) | copy-start | bytes 3145732
  7.2 0.9 copy-start.12
  7.2 15.9 %copy-start.9 = (bf16[512,512]{1,0:T(8,128)(2,1)S(1)}, bf16[512,512]{1,0:T(8,128)(2,1)}, u32[]{:S(2)}) copy-start(bf16[512,512]{1,0:T(8,128)(2,1)} %param.26) | copy-start | bytes 1572868
  7.2 68.7 %all-reduce.27.cloned.1.call-start = ((), (), s32[]{:S(2)}) async-start(), calls=%async_computation.1 | async-start | bytes 164864
  21.2 3.7 %copy-start.3 = (bf16[512,1024]{1,0:T(8,128)(2,1)S(1)}, bf16[512,1024]{1,0:T(8,128)(2,1)}, u32[]{:S(2)}) copy-start(bf16[512,1024]{1,0:T(8,128)(2,1)} %param.27) | copy-start | bytes 3145732
  23.9 113.2 %copy-start.7 = (f32[2,4,256,128]{3,2,1,0:T(8,128)S(1)}, f32[2,4,256,128]{3,2,1,0:T(8,128)}, u32[]{:S(2)}) copy-start(f32[2,4,256,128]{3,2,1,0:T(8,128)} %param.32) | copy-start | bytes 3145732
  24.0 112.3 %all-reduce.31.cloned.1.call-start = ((), (), s32[]{:S(2)}) async-start(), calls=%async_computation.3 | async-start | bytes 131072
  25.8 206.8 %all-reduce.25.cloned.1.call-start = ((), (), s32[]{:S(2)}) async-start(), calls=%async_computation | async-start | bytes 164864
  25.8 0.7 copy-start.25
  26.5 0.7 copy-start.24
  27.2 0.7 copy-start.19
  75.9 0.6 copy-start.22
  78.1 0.7 copy-start.20
  78.9 0.6 copy-start.17
  79.5 0.7 copy-start.15
  137.5 16.3 %copy-start.1 = (f32[2,4,256,128]{3,2,1,0:T(8,128)}, f32[2,4,256,128]{3,2,1,0:T(8,128)S(1)}, u32[]{:S(2)}) copy-start(f32[2,4,256,128]{3,2,1,0:T(8,128)S(1)} %multiply_add_fusion.1) | copy-start | bytes 3145732
  137.5 16.0 %copy-start.4 = (bf16[1024,512]{1,0:T(8,128)(2,1)S(1)}, bf16[1024,512]{1,0:T(8,128)(2,1)}, u32[]{:S(2)}) copy-start(bf16[1024,512]{1,0:T(8,128)(2,1)} %param.31) | copy-start | bytes 3145732
  177.0 0.7 copy-start.13
  177.7 0.7 copy-start.14
  178.4 2.9 copy-start.10
  178.4 3.7 %copy-start.11 = (bf16[512,512]{1,0:T(8,128)(2,1)S(1)}, bf16[512,512]{1,0:T(8,128)(2,1)}, u32[]{:S(2)}) copy-start(bf16[512,512]{1,0:T(8,128)(2,1)} %param.37) | copy-start | bytes 1572868
  179.1 3.9 %copy-start.5 = (bf16[512,1024]{1,0:T(8,128)(2,1)S(1)}, bf16[512,1024]{1,0:T(8,128)(2,1)}, u32[]{:S(2)}) copy-start(bf16[512,1024]{1,0:T(8,128)(2,1)} %param.38) | copy-start | bytes 3145732
  182.1 111.5 %copy-start.8 = (f32[2,4,256,128]{3,2,1,0:T(8,128)S(1)}, f32[2,4,256,128]{3,2,1,0:T(8,128)}, u32[]{:S(2)}) copy-start(f32[2,4,256,128]{3,2,1,0:T(8,128)} %param.43) | copy-start | bytes 3145732
  183.0 109.8 %all-reduce.29.cloned.1.call-start = ((), (), s32[]{:S(2)}) async-start(), calls=%async_computation.2 | async-start | bytes 131072
  232.6 0.6 copy-start.23
  234.9 0.7 copy-start.21
  235.6 0.6 copy-start.18
  236.2 0.7 copy-start.16
  294.0 16.3 %copy-start.2 = (f32[2,4,256,128]{3,2,1,0:T(8,128)}, f32[2,4,256,128]{3,2,1,0:T(8,128)S(1)}, u32[]{:S(2)}) copy-start(f32[2,4,256,128]{3,2,1,0:T(8,128)S(1)} %multiply_add_fusion) | copy-start | bytes 3145732
  294.0 16.0 %copy-start.6 = (bf16[1024,512]{1,0:T(8,128)(2,1)S(1)}, bf16[1024,512]{1,0:T(8,128)(2,1)}, u32[]{:S(2)}) copy-start(bf16[1024,512]{1,0:T(8,128)(2,1)} %param.42) | copy-start | bytes 3145732
Sparse Core Ops, SparseCore 0:
  24.1 51.7 all-reduce.26
  78.2 57.9 all-reduce.30
  183.1 49.4 all-reduce.24
  234.8 57.9 all-reduce.28
where the time goes:
time: 335 us; the launch traced here: 333 us
  waiting for transfers between devices  206 us (61%)
  blocking collectives  77 us (23%)
  matrix products  15.8 us (5%)
  between operations  15.3 us (5%)
  other arithmetic  11.9 us (4%)
  local copies, waits for them, and re-layouts  7.23 us (2%)
    unnamed x8, waiting for transfers between devices  206 us
    unnamed x2, blocking collectives  32 us
    all_gather x2, blocking collectives, cell_step(): lax.all_gather(gated_rows, 'dp', axis=0, tiled=True)  28.2 us
    all_gather x2, blocking collectives, cell_step(): gathered = lax.all_gather(x_shard, 'tp', axis=0, tiled=True)  16.9 us
    dot_general x12, matrix products, project(): return jnp.dot(scaled, weight, preferred_element_type=jnp.float32)  13.4 us
    unnamed x58, local copies, waits for them, and re-layouts  7.1 us
  transfers between devices with their start and end apart: 4, of which 4 were waited for; matrix products, arithmetic and copies ran while one was open for 3% of the time, Pallas kernels for 0%

commit v1 on v0

v1 whole, which is shorter than its diff:
```python
import jax
import jax.numpy as jnp
from jax import lax
from jax.sharding import PartitionSpec as P

eps = 1e-06
LANES = 128
F32 = jnp.float32
BF16 = jnp.bfloat16


def peers(x, axis, size):
    if size <= 4 and size & (size - 1) == 0:
        return [
            lax.ppermute(x, axis, [(i, i ^ k) for i in range(size)])
            for k in range(size - 1, 0, -1)
        ]
    return None


def gather(x, axis, size):
    return lax.all_to_all(
        jnp.broadcast_to(x[None], (size,) + x.shape), axis, 0, 0
    )


def gather_rows(x, axis, size):
    own = peers(x, axis, size)
    if own is None:
        stacked = gather(x, axis, size)
        return stacked.reshape((-1,) + x.shape[1:])
    me = lax.axis_index(axis)
    order = [x] + own[::-1]
    stacked = jnp.zeros((size,) + x.shape, x.dtype)
    for k, piece in enumerate(order):
        stacked = lax.dynamic_update_index_in_dim(stacked, piece, me ^ k, 0)
    return stacked.reshape((-1,) + x.shape[1:])


def sum_over(x, axis, size):
    rounded = x.astype(BF16)
    others = peers(rounded, axis, size)
    if others is None:
        return jnp.sum(gather(rounded, axis, size).astype(F32), axis=0)
    for piece in others:
        x = x + piece.astype(F32)
    return x


def scatter_sum(x, axis, size):
    blocks = x.reshape((size, x.shape[0] // size) + x.shape[1:])
    rounded = blocks.astype(BF16)
    if size <= 4 and size & (size - 1) == 0:
        me = lax.axis_index(axis)
        total = lax.dynamic_index_in_dim(blocks, me, 0, False)
        for k in range(size - 1, 0, -1):
            piece = lax.dynamic_index_in_dim(rounded, me ^ k, 0, False)
            total = total + lax.ppermute(
                piece, axis, [(i, i ^ k) for i in range(size)]
            ).astype(F32)
        return total
    return jnp.sum(lax.all_to_all(rounded, axis, 0, 0).astype(F32), axis=0)


def split(x):
    high = x.astype(BF16)
    return high, (x - high.astype(F32)).astype(BF16)


def cell_step(
    sizes,
    widened,
    gain,
    w_query,
    w_key,
    w_value,
    w_outgate,
    w_input,
    w_forget,
    w_mixing,
    cell_state,
    norm_state,
    stabilizer,
):
    dp = sizes["dp"]
    seq_count, local_heads, dhv, dhk = cell_state.shape
    all_heads = w_input.shape[1]
    width = widened.shape[1] * dp
    squares = jnp.sum(widened * widened, axis=1, keepdims=True)
    scaled = (widened * gain.astype(F32)).astype(BF16)

    def project(weight):
        return jnp.dot(scaled, weight, preferred_element_type=F32)

    small = jnp.concatenate([project(w_input), project(w_forget), squares], axis=1)
    high, low = split(small)
    pad = -(high.shape[1] * 2) % LANES
    payload = jnp.concatenate(
        [project(w).astype(BF16) for w in (w_query, w_key, w_value, w_outgate)]
        + [high, low, jnp.zeros((high.shape[0], pad), BF16)],
        axis=1,
    )
    received = lax.all_to_all(
        payload.reshape(dp, seq_count, payload.shape[1]), "dp", 0, 0
    )
    total = jnp.sum(received.astype(F32), axis=0)
    nk, nv = local_heads * dhk, local_heads * dhv
    base = 2 * (nk + nv)
    wide = 2 * all_heads + 1
    small = total[:, base : base + wide] + total[:, base + wide : base + 2 * wide]
    row_scale = lax.rsqrt(small[:, 2 * all_heads :] / width + eps)
    offset = lax.axis_index("tp") * local_heads
    gates = small * row_scale
    input_pre = lax.dynamic_slice_in_dim(gates, offset, local_heads, 1)
    forget_pre = lax.dynamic_slice_in_dim(gates, offset + all_heads, local_heads, 1)
    queries = (total[:, :nk] * row_scale).reshape(seq_count, local_heads, dhk) * dhk ** (-0.5)
    key_rows = (total[:, nk : 2 * nk] * row_scale).reshape(seq_count, local_heads, dhk)
    value_rows = (total[:, 2 * nk : 2 * nk + nv] * row_scale).reshape(seq_count, local_heads, dhv)
    outgate_pre = total[:, 2 * nk + nv : base] * row_scale
    log_forget = jax.nn.log_sigmoid(forget_pre)
    stab_next = jnp.maximum(log_forget + stabilizer, input_pre)
    retain = jnp.exp(log_forget + stabilizer - stab_next)
    admitted = jnp.exp(input_pre - stab_next)
    cell_next = (
        retain[:, :, None, None] * cell_state
        + admitted[:, :, None, None] * value_rows[:, :, :, None] * key_rows[:, :, None, :]
    )
    norm_next = retain[:, :, None] * norm_state + admitted[:, :, None] * key_rows
    numerator = jnp.einsum("shvd,shd->shv", cell_next, queries, precision=lax.Precision.HIGHEST)
    denominator = jnp.einsum("shd,shd->sh", norm_next, queries, precision=lax.Precision.HIGHEST)
    readout = numerator / jnp.maximum(jnp.abs(denominator), 1.0)[:, :, None]
    gated = (readout.reshape(seq_count, nv) * jax.nn.sigmoid(outgate_pre)).astype(BF16)
    gathered = gather(gated, "dp", dp).reshape(-1, nv)
    partial = jnp.dot(gathered, w_mixing, preferred_element_type=F32)
    return partial, cell_next, norm_next, stab_next


def per_device(sizes, tokens, *args):
    tp = sizes["tp"]
    rows = tokens.shape[0]
    stream = gather_rows(tokens, "tp", tp).astype(F32)
    partial, *first = cell_step(sizes, stream, *args[:11])
    middle = (stream + sum_over(partial, "tp", tp)).astype(BF16)
    partial, *second = cell_step(sizes, middle.astype(F32), *args[11:])
    own = lax.dynamic_slice_in_dim(middle, lax.axis_index("tp") * rows, rows, 0)
    hidden = (own.astype(F32) + scatter_sum(partial, "tp", tp)).astype(BF16)
    return (hidden, *first, *second)


def solution(mesh):
    sizes = dict(mesh.shape)
    weight = P("dp", "tp")
    cell = (
        P("dp"),
        weight,
        weight,
        weight,
        weight,
        P("dp", None),
        P("dp", None),
        P("tp", "dp"),
        P("dp", "tp", None, None),
        P("dp", "tp", None),
        P("dp", "tp"),
    )
    states = cell[-3:]
    return jax.shard_map(
        lambda *args: per_device(sizes, *args),
        mesh=mesh,
        in_specs=(P("tp", "dp"), *cell, *cell),
        out_specs=(P("tp", "dp"), *states, *states),
        check_vma=False,
    )
```

time: 335 us -> 77.9 us (0.23)
  waiting for transfers between devices: 206 us -> 14.9 us
  blocking collectives: 77 us -> 25 us
  starting transfers between devices: 0.16 us -> 16.5 us
  between operations: 15.3 us -> 0.91 us
  matrix products: 15.8 us -> 9.43 us
  other arithmetic: 11.9 us -> 5.88 us
    unnamed x8 -> x0, waiting for transfers between devices: 206 us -> none
    all_gather x4 -> x0, blocking collectives: 45.1 us -> none  [the longest x2 28.2 us: cell_step(): lax.all_gather(gated_rows, 'dp', axis=0, tiled=True)]
    unnamed x2 -> x0, blocking collectives: 32 us -> none
    all_to_all x0 -> x3, blocking collectives: none -> 25 us  [the longest x2 16.2 us: gather(): lax.all_to_all(jnp.broadcast_to(x[None], (size,) + x.shape), axis, 0, 0)]
    ppermute x0 -> x9, starting transfers between devices: none -> 11.6 us  [the longest x6 8.09 us: peers(): lax.ppermute(x, axis, [(i, i ^ k) for i in range(size)])]
    ppermute x0 -> x9, waiting for transfers between devices: none -> 8.56 us  [the longest x6 5.46 us: peers(): lax.ppermute(x, axis, [(i, i ^ k) for i in range(size)])]
    dot_general x14, matrix products: 13.9 us -> 7.47 us  [the longest x12 6.97 us: project(): return jnp.dot(scaled, weight, preferred_element_type=F32)]
    all_to_all x0 -> x1, waiting for transfers between devices: none -> 6.36 us  [cell_step(): lax.all_to_all(payload.reshape(dp, seq_count, payload.shape[1]), 'dp', 0, 0)]
  transfers between devices with their start and end apart: 4 -> 10, of which waited for: 4 -> 8; matrix products, arithmetic and copies ran while one was open for 3% -> 2% of each run, Pallas kernels for 0% -> 0%
where the time goes in v1:
time: 77.9 us; the launch traced here: 77.2 us
  blocking collectives  25 us (32%)
  starting transfers between devices  16.5 us (21%)
  waiting for transfers between devices  14.9 us (19%)
  matrix products  9.43 us (12%)
  other arithmetic  5.88 us (8%)
  local copies, waits for them, and re-layouts  4.54 us (6%)
  between operations  0.91 us (1%)
    all_to_all x2, blocking collectives, gather(): lax.all_to_all(jnp.broadcast_to(x[None], (size,) + x.shape), axis, 0, 0)  16.2 us
    all_to_all x1, blocking collectives, cell_step(): lax.all_to_all(payload.reshape(dp, seq_count, payload.shape[1]), 'dp', 0, 0)  8.75 us
    ppermute x6, starting transfers between devices, peers(): lax.ppermute(x, axis, [(i, i ^ k) for i in range(size)])  8.09 us
    dot_general x12, matrix products, project(): return jnp.dot(scaled, weight, preferred_element_type=F32)  6.97 us
    all_to_all x1, waiting for transfers between devices, cell_step(): lax.all_to_all(payload.reshape(dp, seq_count, payload.shape[1]), 'dp', 0, 0)  6.36 us
    ppermute x6, waiting for transfers between devices, peers(): lax.ppermute(x, axis, [(i, i ^ k) for i in range(size)])  5.46 us
    all_to_all x1, starting transfers between devices, cell_step(): lax.all_to_all(payload.reshape(dp, seq_count, payload.shape[1]), 'dp', 0, 0)  4.88 us
    ppermute x3, starting transfers between devices, scatter_sum(): lax.ppermute(piece, axis, [(i, i ^ k) for i in range(size)]).astype(F32)  3.55 us
  transfers between devices with their start and end apart: 10, of which 8 were waited for; matrix products, arithmetic and copies ran while one was open for 2% of the time, Pallas kernels for 0%

profile of v1, /device:TPU:0, one launch (start us, length us, event | category | flops | bytes accessed | tf_op | source)
XLA Modules:
  0.0 77.2 jit_solution(1594547732097636282)
XLA Ops:
  0.7 3.0 %collective-permute-start = (bf16[4,512]{1,0:T(4,128)(2,1)}, bf16[4,512]{1,0:T(4,128)(2,1)S(1)}, u32[]{:S(2)}, u32[]{:S(2)}) collective-permute-start(bf16[4,512]{1,0:T(4,128)(2,1)} %param.23), channel_id=1, source_target_pairs={{0,8},{8,0},{16,24},{24,16},{1,9},{9,1},{17,25},{25,17},{2,10},{10... | collective-permute-start | bytes 12296 | tf_op jit(solution)/shard_map/ppermute | solution.py:15
  3.7 1.5 %collective-permute-start.2 = (bf16[4,512]{1,0:T(4,128)(2,1)}, bf16[4,512]{1,0:T(4,128)(2,1)S(1)}, u32[]{:S(2)}, u32[]{:S(2)}) collective-permute-start(bf16[4,512]{1,0:T(4,128)(2,1)} %param.23), channel_id=1, source_target_pairs={{0,24},{8,16},{16,8},{24,0},{1,25},{9,17},{17,9},{25,1},{2,26},{10... | collective-permute-start | bytes 12296 | tf_op jit(solution)/shard_map/ppermute | solution.py:15
  5.2 0.7 bitcast_dynamic-update-slice_fusion.3
  6.0 0.7 convert_element_type.113
  6.7 2.3 %collective-permute-done.1 = bf16[4,512]{1,0:T(4,128)(2,1)S(1)} collective-permute-done((bf16[4,512]{1,0:T(4,128)(2,1)}, bf16[4,512]{1,0:T(4,128)(2,1)S(1)}, u32[]{:S(2)}, u32[]{:S(2)}) %collective-permute-start.1) | collective-permute-done | bytes 4128 | tf_op jit(solution)/shard_map/ppermute | solution.py:15
  9.2 0.8 %fusion.43 = f32[16,16]{1,0:T(8,128)S(1)} fusion(bf16[16,512]{1,0:T(8,128)(2,1)S(1)} %multiply_convert_fusion, bf16[512,16]{0,1:T(8,128)(2,1)} %param.30), kind=kOutput, calls=%fused_computation.100 | convolution fusion | flops 262144 | bytes 33792 | tf_op jit(solution)/shard_map/dot_general | solution.py:93
  10.1 0.8 %fusion.42 = f32[16,16]{1,0:T(8,128)S(1)} fusion(bf16[16,512]{1,0:T(8,128)(2,1)S(1)} %multiply_convert_fusion, bf16[512,16]{0,1:T(8,128)(2,1)} %param.29), kind=kOutput, calls=%fused_computation.99 | convolution fusion | flops 262144 | bytes 33792 | tf_op jit(solution)/shard_map/dot_general | solution.py:93
  11.1 1.3 %convolution_convert_fusion.6 = bf16[16,512]{1,0:T(8,128)(2,1)S(1)} fusion(bf16[16,512]{1,0:T(8,128)(2,1)S(1)} %multiply_convert_fusion, bf16[512,512]{1,0:T(8,128)(2,1)} %param.26), kind=kOutput, calls=%fused_computation.6 | convolution fusion | flops 8396800 | bytes 557056 | tf_op jit(solution)/shard_map/dot_general | solution.py:93
  12.4 0.2 convolution_convert_fusion.7
  12.5 0.3 convolution_convert_fusion.2
  12.8 0.3 convolution_convert_fusion.3
  13.2 0.7 reshape.80
  13.9 4.9 %all-to-all-start = ((bf16[8,2,3200]{2,1,0:T(2,128)(2,1)}), bf16[8,2,3200]{2,1,0:T(2,128)(2,1)S(1)}, u32[]{:S(2)}, u32[]{:S(2)}) async-start(bf16[8,2,3200]{2,1,0:T(2,128)(2,1)} %reshape.80), calls=%async_computation | async-start | bytes 204800 | tf_op jit(solution)/shard_map/all_to_all | solution.py:103
  18.7 6.4 %all-to-all-done = bf16[8,2,3200]{2,1,0:T(2,128)(2,1)S(1)} async-done(((bf16[8,2,3200]{2,1,0:T(2,128)(2,1)}), bf16[8,2,3200]{2,1,0:T(2,128)(2,1)S(1)}, u32[]{:S(2)}, u32[]{:S(2)}) %all-to-all-start) | async-done | bytes 102432 | tf_op jit(solution)/shard_map/all_to_all | solution.py:103
  25.3 0.2 rsqrt_reduce_fusion.1
  25.7 0.7 copy-done.18
  26.6 0.5 copy-done.15
  27.2 0.7 multiply_reduce_fusion.2
  27.9 0.4 multiply_add_fusion.1
  28.3 1.0 %fusion.44 = f32[2,4,1,256]{3,2,1,0:T(1,128)S(1)} fusion(f32[2,4,256,128]{3,2,1,0:T(8,128)S(1)} %multiply_add_fusion.1, f32[2,4,128,1]{2,3,1,0:T(1,128)S(1)} %bitcast.74), kind=kOutput, calls=%fused_computation.101 | convolution fusion | flops 3145728 | bytes 1060864 | tf_op jit(solution)/shard_map/shvd,shd->shv/dot_general | solution.py:129
  29.5 8.1 %all_to_all.20 = bf16[8,2,1024]{2,1,0:T(2,128)(2,1)S(1)} all-to-all(bf16[8,2,1024]{2,1,0:T(2,128)(2,1)S(1)} %broadcast_in_dim.52), channel_id=1, replica_groups=mesh['tp'=4,'dp'=8] {'dp'}, dimensions={0} | all-to-all | bytes 65536 | tf_op jit(solution)/shard_map/all_to_all | solution.py:22
  37.7 0.2 fusion.40
  37.9 1.5 %collective-permute-start.5 = (bf16[16,512]{1,0:T(8,128)(2,1)S(1)}, bf16[16,512]{1,0:T(8,128)(2,1)S(1)}, u32[]{:S(2)}, u32[]{:S(2)}) collective-permute-start(bf16[16,512]{1,0:T(8,128)(2,1)S(1)} %get-tuple-element.24), channel_id=1, source_target_pairs={{0,8},{8,0},{16,24},{24,16},{1,9},{9,1},{17,25},{25,17},{2,10},{10... | collective-permute-start | bytes 49160 | tf_op jit(solution)/shard_map/ppermute | solution.py:15
  39.4 0.5 collective-permute-start.4
  39.9 1.5 %collective-permute-start.3 = (bf16[16,512]{1,0:T(8,128)(2,1)S(1)}, bf16[16,512]{1,0:T(8,128)(2,1)S(1)}, u32[]{:S(2)}, u32[]{:S(2)}) collective-permute-start(bf16[16,512]{1,0:T(8,128)(2,1)S(1)} %get-tuple-element.24), channel_id=1, source_target_pairs={{0,24},{8,16},{16,8},{24,0},{1,25},{9,17},{17,9},{25,1},{2,26},{10... | collective-permute-start | bytes 49160 | tf_op jit(solution)/shard_map/ppermute | solution.py:15
  41.4 0.2 collective-permute-done.5
  41.7 1.5 %collective-permute-done.4 = bf16[16,512]{1,0:T(8,128)(2,1)S(1)} collective-permute-done((bf16[16,512]{1,0:T(8,128)(2,1)S(1)}, bf16[16,512]{1,0:T(8,128)(2,1)S(1)}, u32[]{:S(2)}, u32[]{:S(2)}) %collective-permute-start.4) | collective-permute-done | bytes 16416 | tf_op jit(solution)/shard_map/ppermute | solution.py:15
  43.2 1.4 %collective-permute-done.3 = bf16[16,512]{1,0:T(8,128)(2,1)S(1)} collective-permute-done((bf16[16,512]{1,0:T(8,128)(2,1)S(1)}, bf16[16,512]{1,0:T(8,128)(2,1)S(1)}, u32[]{:S(2)}, u32[]{:S(2)}) %collective-permute-start.3) | collective-permute-done | bytes 16416 | tf_op jit(solution)/shard_map/ppermute | solution.py:15
  45.2 1.3 %convolution_convert_fusion.4 = bf16[16,512]{1,0:T(8,128)(2,1)S(1)} fusion(bf16[512,512]{1,0:T(8,128)(2,1)} %param.37, bf16[16,512]{1,0:T(8,128)(2,1)S(1)} %get-tuple-element.12, f32[512]{0:T(512)S(1)} %convert_element_type.132), kind=kOutput, calls=%fused_computation.4 | convolution fusion | flops 8421376 | bytes 559104 | tf_op jit(solution)/shard_map/dot_general | solution.py:93
  46.5 1.2 %convolution_convert_fusion.5 = bf16[16,512]{1,0:T(8,128)(2,1)S(1)} fusion(bf16[512,512]{1,0:T(8,128)(2,1)} %param.36, bf16[16,512]{1,0:T(8,128)(2,1)S(1)} %get-tuple-element.12, f32[512]{0:T(512)S(1)} %convert_element_type.132), kind=kOutput, calls=%fused_computation.5 | convolution fusion | flops 8421376 | bytes 559104 | tf_op jit(solution)/shard_map/dot_general | solution.py:93
  47.7 0.3 convolution_convert_fusion.1
  48.0 0.3 convolution_convert_fusion
  48.4 8.8 %all_to_all.21 = bf16[8,2,3200]{2,1,0:T(2,128)(2,1)S(1)} all-to-all(bf16[8,2,3200]{2,1,0:T(2,128)(2,1)S(1)} %reshape.83), channel_id=1, replica_groups=mesh['tp'=4,'dp'=8] {'dp'}, dimensions={0} | all-to-all | bytes 204800 | tf_op jit(solution)/shard_map/all_to_all | solution.py:103
  57.3 0.2 rsqrt_reduce_fusion
  57.8 0.7 copy-done.19
  58.6 0.5 copy-done.16
  59.2 0.7 multiply_reduce_fusion.1
  59.9 0.4 multiply_add_fusion
  60.3 1.0 %fusion.45 = f32[2,4,1,256]{3,2,1,0:T(1,128)S(1)} fusion(f32[2,4,256,128]{3,2,1,0:T(8,128)S(1)} %multiply_add_fusion, f32[2,4,128,1]{2,3,1,0:T(1,128)S(1)} %bitcast.73), kind=kOutput, calls=%fused_computation.102 | convolution fusion | flops 3145728 | bytes 1060864 | tf_op jit(solution)/shard_map/shvd,shd->shv/dot_general | solution.py:129
  61.5 8.1 %all_to_all.22 = bf16[8,2,1024]{2,1,0:T(2,128)(2,1)S(1)} all-to-all(bf16[8,2,1024]{2,1,0:T(2,128)(2,1)S(1)} %broadcast_in_dim.54), channel_id=1, replica_groups=mesh['tp'=4,'dp'=8] {'dp'}, dimensions={0} | all-to-all | bytes 65536 | tf_op jit(solution)/shard_map/all_to_all | solution.py:22
  69.6 0.3 fusion.41
  69.9 1.6 %collective-permute-start.6 = (bf16[4,512]{1,0:T(4,128)(2,1)S(1)}, bf16[4,512]{1,0:T(4,128)(2,1)S(1)}, u32[]{:S(2)}, u32[]{:S(2)}) collective-permute-start(bf16[4,512]{1,0:T(4,128)(2,1)S(1)} %get-tuple-element.21), channel_id=1, source_target_pairs={{0,24},{8,16},{16,8},{24,0},{1,25},{9,17},{17,9},{25,1},{2,26},{10... | collective-permute-start | bytes 12296 | tf_op jit(solution)/shard_map/ppermute | solution.py:58
  71.5 1.5 %collective-permute-start.8 = (bf16[4,512]{1,0:T(4,128)(2,1)S(1)}, bf16[4,512]{1,0:T(4,128)(2,1)S(1)}, u32[]{:S(2)}, u32[]{:S(2)}) collective-permute-start(bf16[4,512]{1,0:T(4,128)(2,1)S(1)} %get-tuple-element.22), channel_id=1, source_target_pairs={{0,8},{8,0},{16,24},{24,16},{1,9},{9,1},{17,25},{25,17},{2,10},{10... | collective-permute-start | bytes 12296 | tf_op jit(solution)/shard_map/ppermute | solution.py:58
  73.0 0.5 collective-permute-start.7
  73.5 1.0 %collective-permute-done.6 = bf16[4,512]{1,0:T(4,128)(2,1)S(1)} collective-permute-done((bf16[4,512]{1,0:T(4,128)(2,1)S(1)}, bf16[4,512]{1,0:T(4,128)(2,1)S(1)}, u32[]{:S(2)}, u32[]{:S(2)}) %collective-permute-start.6) | collective-permute-done | bytes 4128 | tf_op jit(solution)/shard_map/ppermute | solution.py:58
  74.5 0.6 collective-permute-done.8
  75.1 1.5 %collective-permute-done.7 = bf16[4,512]{1,0:T(4,128)(2,1)S(1)} collective-permute-done((bf16[4,512]{1,0:T(4,128)(2,1)S(1)}, bf16[4,512]{1,0:T(4,128)(2,1)S(1)}, u32[]{:S(2)}, u32[]{:S(2)}) %collective-permute-start.7) | collective-permute-done | bytes 4128 | tf_op jit(solution)/shard_map/ppermute | solution.py:58
  76.6 0.6 fusion.13
  (97 shorter events, 3.3 us)
Async XLA Ops:
  0.6 11.9 %copy-start = (bf16[512,1024]{1,0:T(8,128)(2,1)S(1)}, bf16[512,1024]{1,0:T(8,128)(2,1)}, u32[]{:S(2)}) copy-start(bf16[512,1024]{1,0:T(8,128)(2,1)} %param.28) | copy-start | bytes 3145732
  0.6 11.7 %copy-start.10 = (bf16[512,512]{1,0:T(8,128)(2,1)S(1)}, bf16[512,512]{1,0:T(8,128)(2,1)}, u32[]{:S(2)}) copy-start(bf16[512,512]{1,0:T(8,128)(2,1)} %param.25) | copy-start | bytes 1572868
  0.7 6.0 %collective-permute-start = (bf16[4,512]{1,0:T(4,128)(2,1)}, bf16[4,512]{1,0:T(4,128)(2,1)S(1)}, u32[]{:S(2)}, u32[]{:S(2)}) collective-permute-start(bf16[4,512]{1,0:T(4,128)(2,1)} %param.23), channel_id=1, source_target_pairs={{0,8},{8,0},{16,24},{24,16},{1,9},{9,1},{17,25},{25,17},{2,10},{10... | collective-permute-start | bytes 12296 | tf_op jit(solution)/shard_map/ppermute | solution.py:15
  3.7 5.3 %collective-permute-start.2 = (bf16[4,512]{1,0:T(4,128)(2,1)}, bf16[4,512]{1,0:T(4,128)(2,1)S(1)}, u32[]{:S(2)}, u32[]{:S(2)}) collective-permute-start(bf16[4,512]{1,0:T(4,128)(2,1)} %param.23), channel_id=1, source_target_pairs={{0,24},{8,16},{16,8},{24,0},{1,25},{9,17},{17,9},{25,1},{2,26},{10... | collective-permute-start | bytes 12296 | tf_op jit(solution)/shard_map/ppermute | solution.py:15
  5.2 3.8 %collective-permute-start.1 = (bf16[4,512]{1,0:T(4,128)(2,1)}, bf16[4,512]{1,0:T(4,128)(2,1)S(1)}, u32[]{:S(2)}, u32[]{:S(2)}) collective-permute-start(bf16[4,512]{1,0:T(4,128)(2,1)} %param.23), channel_id=1, source_target_pairs={{0,16},{8,24},{16,0},{24,8},{1,17},{9,25},{17,1},{25,9},{2,18},{10... | collective-permute-start | bytes 12296 | tf_op jit(solution)/shard_map/ppermute | solution.py:15
  11.0 1.8 %copy-start.3 = (bf16[512,1024]{1,0:T(8,128)(2,1)S(1)}, bf16[512,1024]{1,0:T(8,128)(2,1)}, u32[]{:S(2)}) copy-start(bf16[512,1024]{1,0:T(8,128)(2,1)} %param.27) | copy-start | bytes 3145732
  12.8 15.1 %copy-start.8 = (f32[2,4,256,128]{3,2,1,0:T(8,128)S(1)}, f32[2,4,256,128]{3,2,1,0:T(8,128)}, u32[]{:S(2)}) copy-start(f32[2,4,256,128]{3,2,1,0:T(8,128)} %param.32) | copy-start | bytes 3145732
  13.9 11.2 %all-to-all-start = ((bf16[8,2,3200]{2,1,0:T(2,128)(2,1)}), bf16[8,2,3200]{2,1,0:T(2,128)(2,1)S(1)}, u32[]{:S(2)}, u32[]{:S(2)}) async-start(bf16[8,2,3200]{2,1,0:T(2,128)(2,1)} %reshape.80), calls=%async_computation | async-start | bytes 204800 | tf_op jit(solution)/shard_map/all_to_all | solution.py:103
  25.7 0.7 copy-start.18
  26.5 0.6 copy-start.15
  26.5 0.7 copy-start.13
  28.2 9.7 %copy-start.1 = (f32[2,4,256,128]{3,2,1,0:T(8,128)}, f32[2,4,256,128]{3,2,1,0:T(8,128)S(1)}, u32[]{:S(2)}) copy-start(f32[2,4,256,128]{3,2,1,0:T(8,128)S(1)} %multiply_add_fusion.1) | copy-start | bytes 3145732
  28.3 9.4 %copy-start.4 = (bf16[1024,512]{1,0:T(8,128)(2,1)S(1)}, bf16[1024,512]{1,0:T(8,128)(2,1)}, u32[]{:S(2)}) copy-start(bf16[1024,512]{1,0:T(8,128)(2,1)} %param.31) | copy-start | bytes 3145732
  37.6 3.8 %copy-start.17 = (bf16[512]{0:T(512)(128)(2,1)S(1)}, bf16[512]{0:T(512)(128)(2,1)}, u32[]{:S(2)}) copy-start(bf16[512]{0:T(512)(128)(2,1)} %param.35) | copy-start | bytes 3076
  37.6 7.1 %copy-start.11 = (bf16[512,16]{0,1:T(8,128)(2,1)S(1)}, bf16[512,16]{0,1:T(8,128)(2,1)}, u32[]{:S(2)}) copy-start(bf16[512,16]{0,1:T(8,128)(2,1)} %param.40) | copy-start | bytes 49156
  37.6 7.3 %copy-start.12 = (bf16[512,16]{0,1:T(8,128)(2,1)S(1)}, bf16[512,16]{0,1:T(8,128)(2,1)}, u32[]{:S(2)}) copy-start(bf16[512,16]{0,1:T(8,128)(2,1)} %param.41) | copy-start | bytes 49156
  37.9 9.8 %copy-start.5 = (bf16[512,1024]{1,0:T(8,128)(2,1)S(1)}, bf16[512,1024]{1,0:T(8,128)(2,1)}, u32[]{:S(2)}) copy-start(bf16[512,1024]{1,0:T(8,128)(2,1)} %param.38) | copy-start | bytes 3145732
  37.9 3.8 %collective-permute-start.5 = (bf16[16,512]{1,0:T(8,128)(2,1)S(1)}, bf16[16,512]{1,0:T(8,128)(2,1)S(1)}, u32[]{:S(2)}, u32[]{:S(2)}) collective-permute-start(bf16[16,512]{1,0:T(8,128)(2,1)S(1)} %get-tuple-element.24), channel_id=1, source_target_pairs={{0,8},{8,0},{16,24},{24,16},{1,9},{9,1},{17,25},{25,17},{2,10},{10... | collective-permute-start | bytes 49160 | tf_op jit(solution)/shard_map/ppermute | solution.py:15
  39.4 3.7 %collective-permute-start.4 = (bf16[16,512]{1,0:T(8,128)(2,1)S(1)}, bf16[16,512]{1,0:T(8,128)(2,1)S(1)}, u32[]{:S(2)}, u32[]{:S(2)}) collective-permute-start(bf16[16,512]{1,0:T(8,128)(2,1)S(1)} %get-tuple-element.24), channel_id=1, source_target_pairs={{0,16},{8,24},{16,0},{24,8},{1,17},{9,25},{17,1},{25,9},{2,18},{10... | collective-permute-start | bytes 49160 | tf_op jit(solution)/shard_map/ppermute | solution.py:15
  39.9 4.6 %collective-permute-start.3 = (bf16[16,512]{1,0:T(8,128)(2,1)S(1)}, bf16[16,512]{1,0:T(8,128)(2,1)S(1)}, u32[]{:S(2)}, u32[]{:S(2)}) collective-permute-start(bf16[16,512]{1,0:T(8,128)(2,1)S(1)} %get-tuple-element.24), channel_id=1, source_target_pairs={{0,24},{8,16},{16,8},{24,0},{1,25},{9,17},{17,9},{25,1},{2,26},{10... | collective-permute-start | bytes 49160 | tf_op jit(solution)/shard_map/ppermute | solution.py:15
  45.2 2.8 %copy-start.6 = (bf16[512,1024]{1,0:T(8,128)(2,1)S(1)}, bf16[512,1024]{1,0:T(8,128)(2,1)}, u32[]{:S(2)}) copy-start(bf16[512,1024]{1,0:T(8,128)(2,1)} %param.39) | copy-start | bytes 3145732
  48.0 11.9 %copy-start.9 = (f32[2,4,256,128]{3,2,1,0:T(8,128)S(1)}, f32[2,4,256,128]{3,2,1,0:T(8,128)}, u32[]{:S(2)}) copy-start(f32[2,4,256,128]{3,2,1,0:T(8,128)} %param.43) | copy-start | bytes 3145732
  57.2 2.1 %copy-start.14 = (f32[2,4,128]{2,1,0:T(4,128)S(1)}, f32[2,4,128]{2,1,0:T(4,128)}, u32[]{:S(2)}) copy-start(f32[2,4,128]{2,1,0:T(4,128)} %param.44) | copy-start | bytes 12292
  57.8 0.7 copy-start.19
  58.5 0.6 copy-start.16
  60.3 9.6 %copy-start.2 = (f32[2,4,256,128]{3,2,1,0:T(8,128)}, f32[2,4,256,128]{3,2,1,0:T(8,128)S(1)}, u32[]{:S(2)}) copy-start(f32[2,4,256,128]{3,2,1,0:T(8,128)S(1)} %multiply_add_fusion) | copy-start | bytes 3145732
  60.3 9.4 %copy-start.7 = (bf16[1024,512]{1,0:T(8,128)(2,1)S(1)}, bf16[1024,512]{1,0:T(8,128)(2,1)}, u32[]{:S(2)}) copy-start(bf16[1024,512]{1,0:T(8,128)(2,1)} %param.42) | copy-start | bytes 3145732
  69.9 4.6 %collective-permute-start.6 = (bf16[4,512]{1,0:T(4,128)(2,1)S(1)}, bf16[4,512]{1,0:T(4,128)(2,1)S(1)}, u32[]{:S(2)}, u32[]{:S(2)}) collective-permute-start(bf16[4,512]{1,0:T(4,128)(2,1)S(1)} %get-tuple-element.21), channel_id=1, source_target_pairs={{0,24},{8,16},{16,8},{24,0},{1,25},{9,17},{17,9},{25,1},{2,26},{10... | collective-permute-start | bytes 12296 | tf_op jit(solution)/shard_map/ppermute | solution.py:58
  71.5 3.6 %collective-permute-start.8 = (bf16[4,512]{1,0:T(4,128)(2,1)S(1)}, bf16[4,512]{1,0:T(4,128)(2,1)S(1)}, u32[]{:S(2)}, u32[]{:S(2)}) collective-permute-start(bf16[4,512]{1,0:T(4,128)(2,1)S(1)} %get-tuple-element.22), channel_id=1, source_target_pairs={{0,8},{8,0},{16,24},{24,16},{1,9},{9,1},{17,25},{25,17},{2,10},{10... | collective-permute-start | bytes 12296 | tf_op jit(solution)/shard_map/ppermute | solution.py:58
  73.0 3.6 %collective-permute-start.7 = (bf16[4,512]{1,0:T(4,128)(2,1)S(1)}, bf16[4,512]{1,0:T(4,128)(2,1)S(1)}, u32[]{:S(2)}, u32[]{:S(2)}) collective-permute-start(bf16[4,512]{1,0:T(4,128)(2,1)S(1)} %get-tuple-element.23), channel_id=1, source_target_pairs={{0,16},{8,24},{16,0},{24,8},{1,17},{9,25},{17,1},{25,9},{2,18},{10... | collective-permute-start | bytes 12296 | tf_op jit(solution)/shard_map/ppermute | solution.py:58

commit v2 on v1

v2 whole, which is shorter than its diff:
```python
import functools

import jax
import jax.numpy as jnp
from jax import lax
from jax.experimental import pallas as pl
from jax.experimental.pallas import tpu as pltpu
from jax.sharding import PartitionSpec as P

eps = 1e-06
LANES = 128
F32 = jnp.float32
BF16 = jnp.bfloat16
NT = (((1,), (1,)), ((), ()))
TN = (((0,), (0,)), ((), ()))
MIB = 1 << 20


def pairwise(size):
    return size <= 4 and size & (size - 1) == 0


def peers(pieces, axis, size):
    order = sorted(range(1, size), key=lambda k: -bin(k).count("1"))
    got = {}
    for k in order:
        got[k] = lax.ppermute(pieces[k - 1], axis, [(i, i ^ k) for i in range(size)])
    return [got[k] for k in range(1, size)]


def split(x):
    high = x.astype(BF16)
    return high, (x - high.astype(F32)).astype(BF16)


def call(body, outs, scratch, cost, limit, *args):
    return pl.pallas_call(
        body,
        out_shape=outs,
        in_specs=[pl.BlockSpec(memory_space=pltpu.VMEM)] * len(args),
        out_specs=[pl.BlockSpec(memory_space=pltpu.VMEM)] * len(outs),
        scratch_shapes=scratch,
        cost_estimate=pl.CostEstimate(flops=cost, bytes_accessed=cost // 16, transcendentals=0),
        compiler_params=pltpu.CompilerParams(vmem_limit_bytes=limit),
    )(*args)


def pick(blocks, index):
    chosen = blocks[0]
    for j in range(1, len(blocks)):
        chosen = jnp.where(index == j, blocks[j], chosen)
    return chosen


def place(piece_refs, target):
    rows = piece_refs[0].shape[0]
    blocks = [piece[...].astype(F32) for piece in piece_refs]
    me = lax.axis_index("tp")
    for j in range(len(blocks)):
        target[j * rows : (j + 1) * rows, :] = pick(blocks, me ^ j)


def row_blocks(ref, rows):
    return [ref[j * rows : (j + 1) * rows, :] for j in range(ref.shape[0] // rows)]


def project(x, gain_ref, weights, small_ref, payload_ref, y_ref, narrow):
    batch = x.shape[0]
    squares = jnp.sum(x * x, axis=1, keepdims=True)
    scaled = (x * gain_ref[...].astype(F32)).astype(BF16)
    at = 0
    for w_ref in weights:
        width = w_ref.shape[1]
        y_ref[:, at : at + width] = jnp.dot(scaled, w_ref[...], preferred_element_type=F32)
        at += width
    gates = lax.dot_general(scaled, small_ref[...], NT, preferred_element_type=F32)
    lane = lax.broadcasted_iota(jnp.int32, (batch, LANES), 1)
    gates = jnp.where(lane == narrow, squares, gates)
    high = gates.astype(BF16).astype(F32)
    y_ref[:, at : at + LANES] = high
    y_ref[:, at + LANES : at + 2 * LANES] = gates - high
    count, seqs, _ = payload_ref.shape
    for d in range(count):
        payload_ref[d] = y_ref[d * seqs : (d + 1) * seqs, :].astype(BF16)


def first_body(n_pieces, narrow, *refs):
    pieces = refs[:n_pieces]
    gain_ref, wq, wk, wv, wo, small_ref, payload_ref, stream_ref, y_ref = refs[n_pieces:]
    if n_pieces == 1:
        whole = pieces[0][...].astype(F32)
        stream_ref[...] = whole
    else:
        place(pieces, stream_ref)
    project(stream_ref[...], gain_ref, (wq, wk, wv, wo), small_ref, payload_ref, y_ref, narrow)


def second_body(n_pieces, narrow, *refs):
    stream_in, own_ref = refs[:2]
    pieces = refs[2 : 2 + n_pieces]
    gain_ref, wq, wk, wv, wo, small_ref, payload_ref, stream_ref, y_ref = refs[2 + n_pieces :]
    total = own_ref[...]
    for piece in pieces:
        if len(piece.shape) == 3:
            total = total + jnp.sum(piece[...].astype(F32), axis=0)
        else:
            total = total + piece[...].astype(F32)
    x = (stream_in[...] + total).astype(BF16).astype(F32)
    stream_ref[...] = x
    project(x, gain_ref, (wq, wk, wv, wo), small_ref, payload_ref, y_ref, narrow)


def state_body(
    width, received_ref, cell_ref, norm_ref, stab_ref,
    gated_ref, cell_out, norm_out, stab_out, read_ref,
):
    seqs, heads, dhv, dhk = cell_ref.shape
    nk, nv = heads * dhk, heads * dhv
    total = received_ref[0].astype(F32)
    for d in range(1, received_ref.shape[0]):
        total = total + received_ref[d].astype(F32)
    base = 2 * (nk + nv)
    small = total[:, base : base + LANES] + total[:, base + LANES : base + 2 * LANES]
    scale = lax.rsqrt(small[:, 2 * heads : 2 * heads + 1] / width + eps)
    small = small * scale
    input_pre = small[:, :heads]
    forget_pre = small[:, heads : 2 * heads]
    log_forget = jnp.minimum(forget_pre, 0.0) - jnp.log1p(jnp.exp(-jnp.abs(forget_pre)))
    kept = log_forget + stab_ref[...]
    stab_next = jnp.maximum(kept, input_pre)
    stab_out[...] = stab_next
    retain = jnp.exp(kept - stab_next)
    admitted = jnp.exp(input_pre - stab_next)
    queries = total[:, :nk] * (scale * dhk ** (-0.5))
    keys = total[:, nk : 2 * nk] * scale
    values = total[:, 2 * nk : 2 * nk + nv] * scale
    gate = jax.nn.sigmoid(total[:, 2 * nk + nv : base] * scale)
    row = lax.broadcasted_iota(jnp.int32, (8, dhk), 0)
    row_v = lax.broadcasted_iota(jnp.int32, (8, dhv), 0)
    for s in range(seqs):
        for h in range(heads):
            keep = retain[s : s + 1, h : h + 1]
            admit = admitted[s : s + 1, h : h + 1]
            query = queries[s : s + 1, h * dhk : (h + 1) * dhk]
            key = keys[s : s + 1, h * dhk : (h + 1) * dhk]
            value = values[s : s + 1, h * dhv : (h + 1) * dhv] * admit
            norm_next = keep * norm_ref[s, h : h + 1, :] + admit * key
            norm_out[s, h : h + 1, :] = norm_next
            bound = jnp.maximum(jnp.abs(jnp.sum(norm_next * query, axis=1, keepdims=True)), 1.0)
            key_high = key.astype(BF16).astype(F32)
            key_low = key - key_high
            value_high = value.astype(BF16).astype(F32)
            value_low = value - value_high
            left = jnp.where(row_v < 2, value_high, jnp.where(row_v < 4, value_low, 0.0))
            right = jnp.where(row & 1 == 0, key_high, key_low)
            outer = lax.dot_general(
                left.astype(BF16), right.astype(BF16), TN, preferred_element_type=F32
            )
            cell_next = keep * cell_ref[s, h] + outer
            cell_out[s, h] = cell_next
            query_high = query.astype(BF16).astype(F32)
            asks = jnp.where(row == 0, query_high, jnp.where(row == 1, query - query_high, 0.0))
            asks = asks.astype(BF16)
            cell_high = cell_next.astype(BF16)
            read = lax.dot_general(asks, cell_high, NT, preferred_element_type=F32)
            low = (cell_next - cell_high.astype(F32)).astype(BF16)
            read = read + lax.dot_general(asks, low, NT, preferred_element_type=F32)
            numerator = jnp.sum(read, axis=0, keepdims=True)
            read_ref[s : s + 1, h * dhv : (h + 1) * dhv] = numerator / bound
    gated = (read_ref[...] * gate).astype(BF16)
    for d in range(gated_ref.shape[0]):
        gated_ref[d] = gated


def mix(gathered_ref, w_ref, x_ref):
    count, seqs, _ = gathered_ref.shape
    for d in range(count):
        x_ref[d * seqs : (d + 1) * seqs, :] = gathered_ref[d].astype(F32)
    return jnp.dot(x_ref[...].astype(BF16), w_ref[...], preferred_element_type=F32)


def middle_body(gathered_ref, w_ref, sent_ref, own_ref, x_ref):
    partial = mix(gathered_ref, w_ref, x_ref)
    own_ref[...] = partial
    sent_ref[...] = partial.astype(BF16)


def last_body(paired, size, gathered_ref, w_ref, *refs):
    x_ref, y_ref = refs[-2:]
    y_ref[...] = mix(gathered_ref, w_ref, x_ref)
    if not paired:
        sent_ref = refs[0]
        rows = sent_ref.shape[1]
        for k in range(size):
            sent_ref[k] = y_ref[k * rows : (k + 1) * rows, :].astype(BF16)
        return
    rows = refs[0].shape[0]
    blocks = row_blocks(y_ref, rows)
    me = lax.axis_index("tp")
    for k in range(size):
        refs[k][...] = pick(blocks, me ^ k).astype(refs[k].dtype)


def final_body(stream_ref, *refs):
    hidden_ref = refs[-1]
    rows = hidden_ref.shape[0]
    total = pick(row_blocks(stream_ref, rows), lax.axis_index("tp"))
    for piece in refs[:-1]:
        if len(piece.shape) == 3:
            total = total + jnp.sum(piece[...].astype(F32), axis=0)
        else:
            total = total + piece[...].astype(F32)
    hidden_ref[...] = total.astype(BF16)


def own_gates(w_input, w_forget, heads):
    offset = lax.axis_index("tp") * heads
    rows = jnp.concatenate(
        [lax.dynamic_slice_in_dim(w.T, offset, heads, 0) for w in (w_input, w_forget)], axis=0
    )
    return jnp.pad(rows, ((0, LANES - rows.shape[0]), (0, 0)))


def per_device(sizes, tokens, *args):
    tp, dp = sizes["tp"], sizes["dp"]
    paired = pairwise(tp)
    rows, features = tokens.shape
    batch = rows * tp
    cells = (args[:11], args[11:])
    seqs, heads, dhv, dhk = cells[0][8].shape
    nk, nv = heads * dhk, heads * dhv
    payload_width = 2 * (nk + nv) + 2 * LANES
    payload = jax.ShapeDtypeStruct((dp, seqs, payload_width), BF16)
    stream = jax.ShapeDtypeStruct((batch, features), F32)
    gated = jax.ShapeDtypeStruct((dp, seqs, nv), BF16)
    small = [own_gates(cell[5], cell[6], heads) for cell in cells]
    gains = [cell[0].reshape(1, features) for cell in cells]
    project_scratch = [pltpu.VMEM((batch, payload_width), F32)]
    project_cost = 2 * batch * features * payload_width
    mix_scratch = pltpu.VMEM((batch, nv), F32)
    mix_cost = 2 * batch * features * nv
    state_cost = 16 * seqs * nv * dhk

    def exchange_dp(x):
        return lax.all_to_all(x, "dp", 0, 0)

    def update(received, cell):
        return call(
            functools.partial(state_body, features * dp),
            [
                gated,
                jax.ShapeDtypeStruct(cell[8].shape, F32),
                jax.ShapeDtypeStruct(cell[9].shape, F32),
                jax.ShapeDtypeStruct(cell[10].shape, F32),
            ],
            [pltpu.VMEM((seqs, nv), F32)],
            state_cost,
            12 * MIB,
            received,
            *cell[8:],
        )

    if paired:
        pieces = [tokens] + peers([tokens] * (tp - 1), "tp", tp)
    else:
        stacked = lax.all_to_all(jnp.broadcast_to(tokens[None], (tp, rows, features)), "tp", 0, 0)
        pieces = [stacked.reshape(batch, features)]
    sums, x = call(
        functools.partial(first_body, len(pieces), 2 * heads),
        [payload, stream],
        project_scratch,
        project_cost,
        12 * MIB,
        *pieces,
        gains[0],
        *cells[0][1:5],
        small[0],
    )
    shared, *first = update(exchange_dp(sums), cells[0])
    sent, own = call(
        middle_body,
        [jax.ShapeDtypeStruct((batch, features), BF16), stream],
        [mix_scratch],
        mix_cost,
        8 * MIB,
        exchange_dp(shared),
        cells[0][7],
    )
    if paired:
        pieces = peers([sent] * (tp - 1), "tp", tp)
    else:
        own = jnp.zeros_like(own)
        pieces = [lax.all_to_all(jnp.broadcast_to(sent[None], (tp, batch, features)), "tp", 0, 0)]
    sums, x = call(
        functools.partial(second_body, len(pieces), 2 * heads),
        [payload, stream],
        project_scratch,
        project_cost,
        12 * MIB,
        x,
        own,
        *pieces,
        gains[1],
        *cells[1][1:5],
        small[1],
    )
    shared, *second = update(exchange_dp(sums), cells[1])
    block = jax.ShapeDtypeStruct((rows, features), BF16)
    if paired:
        outs = [jax.ShapeDtypeStruct((rows, features), F32)] + [block] * (tp - 1)
    else:
        outs = [jax.ShapeDtypeStruct((tp, rows, features), BF16)]
    sent = call(
        functools.partial(last_body, paired, tp),
        outs,
        [mix_scratch, pltpu.VMEM((batch, features), F32)],
        mix_cost,
        8 * MIB,
        exchange_dp(shared),
        cells[1][7],
    )
    if paired:
        pieces = [sent[0]] + peers(sent[1:], "tp", tp)
    else:
        pieces = [lax.all_to_all(sent[0], "tp", 0, 0)]
    (hidden,) = call(final_body, [block], [], rows * features, 2 * MIB, x, *pieces)
    return (hidden, *first, *second)


def solution(mesh):
    sizes = dict(mesh.shape)
    weight = P("dp", "tp")
    cell = (
        P("dp"),
        weight,
        weight,
        weight,
        weight,
        P("dp", None),
        P("dp", None),
        P("tp", "dp"),
        P("dp", "tp", None, None),
        P("dp", "tp", None),
        P("dp", "tp"),
    )
    states = cell[-3:]
    return jax.shard_map(
        lambda *args: per_device(sizes, *args),
        mesh=mesh,
        in_specs=(P("tp", "dp"), *cell, *cell),
        out_specs=(P("tp", "dp"), *states, *states),
        check_vma=False,
    )
```

time: 77.9 us -> 73.6 us (0.945)
  matrix products: 9.43 us -> 0 us
  Pallas kernels: 0 us -> 6.73 us
  other arithmetic: 5.88 us -> 0.02 us
  local copies, waits for them, and re-layouts: 4.54 us -> 9.44 us
  blocking collectives: 25 us -> 28.1 us
  waiting for transfers between devices: 14.9 us -> 12.8 us
  starting transfers between devices: 16.5 us -> 15 us
    dot_general x16 -> x0, matrix products: 9.43 us -> none  [the longest x12 6.97 us: project(): return jnp.dot(scaled, weight, preferred_element_type=F32)]
    pallas_call x0 -> x7, Pallas kernels: none -> 6.73 us  [call(): pl.pallas_call(body, out_shape=outs, in_specs=[pl.BlockSpec(memory_space=...]
    unnamed x42 -> x38, local copies, waits for them, and re-layouts: 2.43 us -> 7.98 us
    all_to_all x3, blocking collectives: 25 us -> 28.1 us  [exchange_dp(): return lax.all_to_all(x, 'dp', 0, 0)]
    convert_element_type x10 -> x0, other arithmetic: 1.8 us -> none  [the longest x3 0.69 us: cell_step(): scaled = (widened * gain.astype(F32)).astype(BF16)]
    all_to_all x1, starting transfers between devices: 4.88 us -> 3.34 us  [exchange_dp(): return lax.all_to_all(x, 'dp', 0, 0)]
    dynamic_slice x0 -> x2, local copies, waits for them, and re-layouts: none -> 1.45 us  [own_gates(): lax.dynamic_slice_in_dim(w.T, offset, heads, 0)]
    all_to_all x1, waiting for transfers between devices: 6.36 us -> 4.94 us  [exchange_dp(): return lax.all_to_all(x, 'dp', 0, 0)]
where the time goes in v2:
time: 73.6 us; the launch traced here: 72.9 us
  blocking collectives  28.1 us (38%)
  starting transfers between devices  15 us (20%)
  waiting for transfers between devices  12.8 us (17%)
  local copies, waits for them, and re-layouts  9.44 us (13%)
  Pallas kernels  6.73 us (9%)
  between operations  0.76 us (1%)
    all_to_all x3, blocking collectives, exchange_dp(): return lax.all_to_all(x, 'dp', 0, 0)  28.1 us
    ppermute x9, starting transfers between devices, peers(): lax.ppermute(pieces[k - 1], axis, [(i, i ^ k) for i in range(size)])  11.7 us
    unnamed x38, local copies, waits for them, and re-layouts  7.98 us
    ppermute x9, waiting for transfers between devices, peers(): lax.ppermute(pieces[k - 1], axis, [(i, i ^ k) for i in range(size)])  7.84 us
    pallas_call x7, Pallas kernels, call(): pl.pallas_call(body, out_shape=outs, in_specs=[pl.BlockSpec(memory_space=...  6.73 us
    all_to_all x1, waiting for transfers between devices, exchange_dp(): return lax.all_to_all(x, 'dp', 0, 0)  4.94 us
    all_to_all x1, starting transfers between devices, exchange_dp(): return lax.all_to_all(x, 'dp', 0, 0)  3.34 us
  transfers between devices with their start and end apart: 10, of which 8 were waited for; matrix products, arithmetic and copies ran while one was open for 2% of the time, Pallas kernels for 0%

profile of v2, /device:TPU:0, one launch (start us, length us, event | category | flops | bytes accessed | tf_op | source)
XLA Modules:
  0.0 72.9 jit_solution(10741097711234887636)
XLA Ops:
  0.6 3.1 %collective-permute-start.1 = (bf16[4,512]{1,0:T(4,128)(2,1)}, bf16[4,512]{1,0:T(4,128)(2,1)S(1)}, u32[]{:S(2)}, u32[]{:S(2)}) collective-permute-start(bf16[4,512]{1,0:T(4,128)(2,1)} %refs_0_.1), channel_id=1, source_target_pairs={{0,16},{8,24},{16,0},{24,8},{1,17},{9,25},{17,1},{25,9},{2,18},{10... | collective-permute-start | bytes 12296 | tf_op jit(solution)/shard_map/ppermute | solution.py:27
  3.7 1.5 %collective-permute-start = (bf16[4,512]{1,0:T(4,128)(2,1)}, bf16[4,512]{1,0:T(4,128)(2,1)S(1)}, u32[]{:S(2)}, u32[]{:S(2)}) collective-permute-start(bf16[4,512]{1,0:T(4,128)(2,1)} %refs_0_.1), channel_id=1, source_target_pairs={{0,8},{8,0},{16,24},{24,16},{1,9},{9,1},{17,25},{25,17},{2,10},{10... | collective-permute-start | bytes 12296 | tf_op jit(solution)/shard_map/ppermute | solution.py:27
  5.2 0.1 collective-permute-start.2
  5.2 0.7 dynamic-slice_bitcast_fusion.2
  6.0 0.0 copy-start.12
  6.0 0.6 copy-done.17
  6.6 0.0 collective-permute-done.1.refs_2_
  6.7 0.9 %collective-permute-done.refs_1_ = bf16[4,512]{1,0:T(4,128)(2,1)S(1)} collective-permute-done((bf16[4,512]{1,0:T(4,128)(2,1)}, bf16[4,512]{1,0:T(4,128)(2,1)S(1)}, u32[]{:S(2)}, u32[]{:S(2)}) %collective-permute-start) | collective-permute-done | bytes 4128 | tf_op jit(solution)/shard_map/ppermute | solution.py:27
  7.5 2.4 %collective-permute-done.2.refs_3_ = bf16[4,512]{1,0:T(4,128)(2,1)S(1)} collective-permute-done((bf16[4,512]{1,0:T(4,128)(2,1)}, bf16[4,512]{1,0:T(4,128)(2,1)S(1)}, u32[]{:S(2)}, u32[]{:S(2)}) %collective-permute-start.2) | collective-permute-done | bytes 4128 | tf_op jit(solution)/shard_map/ppermute | solution.py:27
  9.9 1.2 %copy-done.6 = bf16[512,1024]{1,0:T(8,128)(2,1)S(1)} copy-done((bf16[512,1024]{1,0:T(8,128)(2,1)S(1)}, bf16[512,1024]{1,0:T(8,128)(2,1)}, u32[]{:S(2)}) %copy-start.6) | copy-done | bytes 1048600
  11.1 1.2 %copy-done.7 = bf16[512,1024]{1,0:T(8,128)(2,1)S(1)} copy-done((bf16[512,1024]{1,0:T(8,128)(2,1)S(1)}, bf16[512,1024]{1,0:T(8,128)(2,1)}, u32[]{:S(2)}) %copy-start.7) | copy-done | bytes 1048600
  12.4 1.0 %copy-done.8 = bf16[512,512]{1,0:T(8,128)(2,1)S(1)} copy-done((bf16[512,512]{1,0:T(8,128)(2,1)S(1)}, bf16[512,512]{1,0:T(8,128)(2,1)}, u32[]{:S(2)}) %copy-start.8) | copy-done | bytes 524312
  13.4 1.0 %copy-done.9 = bf16[512,512]{1,0:T(8,128)(2,1)S(1)} copy-done((bf16[512,512]{1,0:T(8,128)(2,1)S(1)}, bf16[512,512]{1,0:T(8,128)(2,1)}, u32[]{:S(2)}) %copy-start.9) | copy-done | bytes 524312
  14.4 0.6 shard_map.270
  15.0 0.0 copy-start.13
  15.1 0.0 copy-start.15
  15.1 11.1 %all_to_all.20.received_ref = bf16[8,2,3328]{2,1,0:T(2,128)(2,1)S(1)} all-to-all(bf16[8,2,3328]{2,1,0:T(2,128)(2,1)S(1)} %get-tuple-element.26), channel_id=1, replica_groups=mesh['tp'=4,'dp'=8] {'dp'}, dimensions={0} | all-to-all | bytes 212992 | tf_op jit(solution)/shard_map/all_to_all | solution.py:245
  26.2 0.0 copy-done.15
  26.2 0.0 copy-start
  26.2 0.0 copy-start.1
  26.2 2.2 %shard_map.271 = (bf16[8,2,1024]{2,1,0:T(2,128)(2,1)}, f32[2,4,256,128]{3,2,1,0:T(8,128)}, f32[2,4,128]{2,1,0:T(4,128)}, f32[2,4]{1,0:T(2,128)}) custom-call(bf16[8,2,3328]{2,1,0:T(2,128)(2,1)S(1)} %all_to_all.20.received_ref, f32[2,4,256,128]{3,2,1,0:T(8,128)S(1)} %copy-done.2, f32[2,4,128]{2,1,0:T(4,128)S(1)} %copy-done.13, f32[2,4]{1,0:T(2,128)S(1)} %copy-done.15), custom_call_target="tpu_custom_call" | custom-call | flops 4194304 | bytes 262144 | tf_op jit(solution)/shard_map/pallas_call | solution.py:37
  28.4 3.3 %all-to-all-start.1 = ((bf16[8,2,1024]{2,1,0:T(2,128)(2,1)}), bf16[8,2,1024]{2,1,0:T(2,128)(2,1)S(1)}, u32[]{:S(2)}, u32[]{:S(2)}) async-start(bf16[8,2,1024]{2,1,0:T(2,128)(2,1)} %get-tuple-element.27), calls=%async_computation.1 | async-start | bytes 65536 | tf_op jit(solution)/shard_map/all_to_all | solution.py:245
  31.8 0.7 %dynamic-slice_bitcast_fusion = (bf16[4,512]{1,0:T(4,128)(2,1)S(1)}, bf16[4,512]{1,0:T(4,128)(2,1)S(1)}) fusion(bf16[512,16]{0,1:T(8,128)(2,1)} %param.41, s32[]{:T(128)S(6)} %select_n.2, bf16[512,16]{0,1:T(8,128)(2,1)} %param.40), kind=kLoop, calls=%fused_computation.7 | loop fusion | bytes 16388 | tf_op jit(solution)/shard_map/dynamic_slice | solution.py:219
  32.5 4.9 %all-to-all-done.1.gathered_ref = bf16[8,2,1024]{2,1,0:T(2,128)(2,1)S(1)} async-done(((bf16[8,2,1024]{2,1,0:T(2,128)(2,1)}), bf16[8,2,1024]{2,1,0:T(2,128)(2,1)S(1)}, u32[]{:S(2)}, u32[]{:S(2)}) %all-to-all-start.1) | async-done | bytes 32800 | tf_op jit(solution)/shard_map/all_to_all | solution.py:245
  37.4 0.2 shard_map.272
  37.7 0.5 collective-permute-start.5
  38.2 1.5 %collective-permute-start.4 = (bf16[16,512]{1,0:T(8,128)(2,1)S(1)}, bf16[16,512]{1,0:T(8,128)(2,1)S(1)}, u32[]{:S(2)}, u32[]{:S(2)}) collective-permute-start(bf16[16,512]{1,0:T(8,128)(2,1)S(1)} %get-tuple-element.29), channel_id=1, source_target_pairs={{0,16},{8,24},{16,0},{24,8},{1,17},{9,25},{17,1},{25,9},{2,18},{10... | collective-permute-start | bytes 49160 | tf_op jit(solution)/shard_map/ppermute | solution.py:27
  39.7 1.5 %collective-permute-start.3 = (bf16[16,512]{1,0:T(8,128)(2,1)S(1)}, bf16[16,512]{1,0:T(8,128)(2,1)S(1)}, u32[]{:S(2)}, u32[]{:S(2)}) collective-permute-start(bf16[16,512]{1,0:T(8,128)(2,1)S(1)} %get-tuple-element.29), channel_id=1, source_target_pairs={{0,8},{8,0},{16,24},{24,16},{1,9},{9,1},{17,25},{25,17},{2,10},{10... | collective-permute-start | bytes 49160 | tf_op jit(solution)/shard_map/ppermute | solution.py:27
  41.2 0.7 copy-done.18
  41.9 0.5 collective-permute-done.5.refs_4_
  42.3 0.0 collective-permute-done.4.refs_3_
  42.3 1.1 %collective-permute-done.3.refs_2_ = bf16[16,512]{1,0:T(8,128)(2,1)S(1)} collective-permute-done((bf16[16,512]{1,0:T(8,128)(2,1)S(1)}, bf16[16,512]{1,0:T(8,128)(2,1)S(1)}, u32[]{:S(2)}, u32[]{:S(2)}) %collective-permute-start.3) | collective-permute-done | bytes 16416 | tf_op jit(solution)/shard_map/ppermute | solution.py:27
  43.4 0.0 copy-done.1
  43.4 1.0 %copy-done.10 = bf16[512,512]{1,0:T(8,128)(2,1)S(1)} copy-done((bf16[512,512]{1,0:T(8,128)(2,1)S(1)}, bf16[512,512]{1,0:T(8,128)(2,1)}, u32[]{:S(2)}) %copy-start.10) | copy-done | bytes 524312
  44.5 1.0 %copy-done.11 = bf16[512,512]{1,0:T(8,128)(2,1)S(1)} copy-done((bf16[512,512]{1,0:T(8,128)(2,1)S(1)}, bf16[512,512]{1,0:T(8,128)(2,1)}, u32[]{:S(2)}) %copy-start.11) | copy-done | bytes 524312
  45.5 0.6 shard_map.273
  46.1 0.0 copy-start.5
  46.1 8.9 %all_to_all.21.received_ref = bf16[8,2,3328]{2,1,0:T(2,128)(2,1)S(1)} all-to-all(bf16[8,2,3328]{2,1,0:T(2,128)(2,1)S(1)} %get-tuple-element.31), channel_id=1, replica_groups=mesh['tp'=4,'dp'=8] {'dp'}, dimensions={0} | all-to-all | bytes 212992 | tf_op jit(solution)/shard_map/all_to_all | solution.py:245
  55.1 2.2 %shard_map.274 = (bf16[8,2,1024]{2,1,0:T(2,128)(2,1)S(1)}, f32[2,4,256,128]{3,2,1,0:T(8,128)}, f32[2,4,128]{2,1,0:T(4,128)}, f32[2,4]{1,0:T(2,128)}) custom-call(bf16[8,2,3328]{2,1,0:T(2,128)(2,1)S(1)} %all_to_all.21.received_ref, f32[2,4,256,128]{3,2,1,0:T(8,128)S(1)} %copy-done.4, f32[2,4,128]{2,1,0:T(4,128)S(1)} %copy-done.14, f32[2,4]{1,0:T(2,128)S(1)} %copy-done.16), custom_call_target="tpu_custom_call" | custom-call | flops 4194304 | bytes 262144 | tf_op jit(solution)/shard_map/pallas_call | solution.py:37
  57.3 8.1 %all_to_all.22.gathered_ref = bf16[8,2,1024]{2,1,0:T(2,128)(2,1)S(1)} all-to-all(bf16[8,2,1024]{2,1,0:T(2,128)(2,1)S(1)} %get-tuple-element.32), channel_id=1, replica_groups=mesh['tp'=4,'dp'=8] {'dp'}, dimensions={0} | all-to-all | bytes 65536 | tf_op jit(solution)/shard_map/all_to_all | solution.py:245
  65.4 0.3 shard_map.275
  65.7 1.5 %collective-permute-start.6 = (bf16[4,512]{1,0:T(4,128)(2,1)S(1)}, bf16[4,512]{1,0:T(4,128)(2,1)S(1)}, u32[]{:S(2)}, u32[]{:S(2)}) collective-permute-start(bf16[4,512]{1,0:T(4,128)(2,1)S(1)} %get-tuple-element.34), channel_id=1, source_target_pairs={{0,8},{8,0},{16,24},{24,16},{1,9},{9,1},{17,25},{25,17},{2,10},{10... | collective-permute-start | bytes 12296 | tf_op jit(solution)/shard_map/ppermute | solution.py:27
  67.2 0.5 collective-permute-start.7
  67.7 1.5 %collective-permute-start.8 = (bf16[4,512]{1,0:T(4,128)(2,1)S(1)}, bf16[4,512]{1,0:T(4,128)(2,1)S(1)}, u32[]{:S(2)}, u32[]{:S(2)}) collective-permute-start(bf16[4,512]{1,0:T(4,128)(2,1)S(1)} %get-tuple-element.36), channel_id=1, source_target_pairs={{0,24},{8,16},{16,8},{24,0},{1,25},{9,17},{17,9},{25,1},{2,26},{10... | collective-permute-start | bytes 12296 | tf_op jit(solution)/shard_map/ppermute | solution.py:27
  69.2 0.1 collective-permute-done.6.refs_1_
  69.4 1.5 %collective-permute-done.7.refs_2_ = bf16[4,512]{1,0:T(4,128)(2,1)S(1)} collective-permute-done((bf16[4,512]{1,0:T(4,128)(2,1)S(1)}, bf16[4,512]{1,0:T(4,128)(2,1)S(1)}, u32[]{:S(2)}, u32[]{:S(2)}) %collective-permute-start.7) | collective-permute-done | bytes 4128 | tf_op jit(solution)/shard_map/ppermute | solution.py:27
  70.8 1.4 %collective-permute-done.8.refs_3_ = bf16[4,512]{1,0:T(4,128)(2,1)S(1)} collective-permute-done((bf16[4,512]{1,0:T(4,128)(2,1)S(1)}, bf16[4,512]{1,0:T(4,128)(2,1)S(1)}, u32[]{:S(2)}, u32[]{:S(2)}) %collective-permute-start.8) | collective-permute-done | bytes 4128 | tf_op jit(solution)/shard_map/ppermute | solution.py:27
  72.3 0.6 shard_map.276
  (26 shorter events, 0.1 us)
Async XLA Ops:
  0.6 6.0 %collective-permute-start.1 = (bf16[4,512]{1,0:T(4,128)(2,1)}, bf16[4,512]{1,0:T(4,128)(2,1)S(1)}, u32[]{:S(2)}, u32[]{:S(2)}) collective-permute-start(bf16[4,512]{1,0:T(4,128)(2,1)} %refs_0_.1), channel_id=1, source_target_pairs={{0,16},{8,24},{16,0},{24,8},{1,17},{9,25},{17,1},{25,9},{2,18},{10... | collective-permute-start | bytes 12296 | tf_op jit(solution)/shard_map/ppermute | solution.py:27
  3.7 3.8 %collective-permute-start = (bf16[4,512]{1,0:T(4,128)(2,1)}, bf16[4,512]{1,0:T(4,128)(2,1)S(1)}, u32[]{:S(2)}, u32[]{:S(2)}) collective-permute-start(bf16[4,512]{1,0:T(4,128)(2,1)} %refs_0_.1), channel_id=1, source_target_pairs={{0,8},{8,0},{16,24},{24,16},{1,9},{9,1},{17,25},{25,17},{2,10},{10... | collective-permute-start | bytes 12296 | tf_op jit(solution)/shard_map/ppermute | solution.py:27
  5.2 4.7 %collective-permute-start.2 = (bf16[4,512]{1,0:T(4,128)(2,1)}, bf16[4,512]{1,0:T(4,128)(2,1)S(1)}, u32[]{:S(2)}, u32[]{:S(2)}) collective-permute-start(bf16[4,512]{1,0:T(4,128)(2,1)} %refs_0_.1), channel_id=1, source_target_pairs={{0,24},{8,16},{16,8},{24,0},{1,25},{9,17},{17,9},{25,1},{2,26},{10... | collective-permute-start | bytes 12296 | tf_op jit(solution)/shard_map/ppermute | solution.py:27
  6.0 0.7 copy-start.17
  6.0 3.9 %copy-start.12 = (bf16[4,512]{1,0:T(4,128)(2,1)S(1)}, bf16[4,512]{1,0:T(4,128)(2,1)}, u32[]{:S(2)}) copy-start(bf16[4,512]{1,0:T(4,128)(2,1)} %refs_0_.1) | copy-start | bytes 12292
  6.6 19.5 %copy-start.2 = (f32[2,4,256,128]{3,2,1,0:T(8,128)S(1)}, f32[2,4,256,128]{3,2,1,0:T(8,128)}, u32[]{:S(2)}) copy-start(f32[2,4,256,128]{3,2,1,0:T(8,128)} %cell_ref.2) | copy-start | bytes 3145732
  9.9 1.2 %copy-start.6 = (bf16[512,1024]{1,0:T(8,128)(2,1)S(1)}, bf16[512,1024]{1,0:T(8,128)(2,1)}, u32[]{:S(2)}) copy-start(bf16[512,1024]{1,0:T(8,128)(2,1)} %refs_7_.2) | copy-start | bytes 3145732
  11.1 1.2 %copy-start.7 = (bf16[512,1024]{1,0:T(8,128)(2,1)S(1)}, bf16[512,1024]{1,0:T(8,128)(2,1)}, u32[]{:S(2)}) copy-start(bf16[512,1024]{1,0:T(8,128)(2,1)} %refs_8_.2) | copy-start | bytes 3145732
  12.4 1.0 %copy-start.8 = (bf16[512,512]{1,0:T(8,128)(2,1)S(1)}, bf16[512,512]{1,0:T(8,128)(2,1)}, u32[]{:S(2)}) copy-start(bf16[512,512]{1,0:T(8,128)(2,1)} %refs_5_.1) | copy-start | bytes 1572868
  13.4 1.0 %copy-start.9 = (bf16[512,512]{1,0:T(8,128)(2,1)S(1)}, bf16[512,512]{1,0:T(8,128)(2,1)}, u32[]{:S(2)}) copy-start(bf16[512,512]{1,0:T(8,128)(2,1)} %refs_6_.2) | copy-start | bytes 1572868
  14.4 23.0 %copy-start.3 = (bf16[1024,512]{1,0:T(8,128)(2,1)S(1)}, bf16[1024,512]{1,0:T(8,128)(2,1)}, u32[]{:S(2)}) copy-start(bf16[1024,512]{1,0:T(8,128)(2,1)} %w_ref.2) | copy-start | bytes 3145732
  15.0 11.1 %copy-start.13 = (f32[2,4,128]{2,1,0:T(4,128)S(1)}, f32[2,4,128]{2,1,0:T(4,128)}, u32[]{:S(2)}) copy-start(f32[2,4,128]{2,1,0:T(4,128)} %norm_ref.2) | copy-start | bytes 12292
  15.1 11.1 %copy-start.15 = (f32[2,4]{1,0:T(2,128)S(1)}, f32[2,4]{1,0:T(2,128)}, u32[]{:S(2)}) copy-start(f32[2,4]{1,0:T(2,128)} %stab_ref.2) | copy-start | bytes 100
  26.2 17.3 %copy-start = (bf16[512,1024]{1,0:T(8,128)(2,1)S(1)}, bf16[512,1024]{1,0:T(8,128)(2,1)}, u32[]{:S(2)}) copy-start(bf16[512,1024]{1,0:T(8,128)(2,1)} %refs_8_.3) | copy-start | bytes 3145732
  26.2 17.3 %copy-start.1 = (bf16[512,1024]{1,0:T(8,128)(2,1)S(1)}, bf16[512,1024]{1,0:T(8,128)(2,1)}, u32[]{:S(2)}) copy-start(bf16[512,1024]{1,0:T(8,128)(2,1)} %refs_9_.1) | copy-start | bytes 3145732
  28.4 9.0 %all-to-all-start.1 = ((bf16[8,2,1024]{2,1,0:T(2,128)(2,1)}), bf16[8,2,1024]{2,1,0:T(2,128)(2,1)S(1)}, u32[]{:S(2)}, u32[]{:S(2)}) async-start(bf16[8,2,1024]{2,1,0:T(2,128)(2,1)} %get-tuple-element.27), calls=%async_computation.1 | async-start | bytes 65536 | tf_op jit(solution)/shard_map/all_to_all | solution.py:245
  37.7 4.7 %collective-permute-start.5 = (bf16[16,512]{1,0:T(8,128)(2,1)S(1)}, bf16[16,512]{1,0:T(8,128)(2,1)S(1)}, u32[]{:S(2)}, u32[]{:S(2)}) collective-permute-start(bf16[16,512]{1,0:T(8,128)(2,1)S(1)} %get-tuple-element.29), channel_id=1, source_target_pairs={{0,24},{8,16},{16,8},{24,0},{1,25},{9,17},{17,9},{25,1},{2,26},{10... | collective-permute-start | bytes 49160 | tf_op jit(solution)/shard_map/ppermute | solution.py:27
  38.2 4.2 %collective-permute-start.4 = (bf16[16,512]{1,0:T(8,128)(2,1)S(1)}, bf16[16,512]{1,0:T(8,128)(2,1)S(1)}, u32[]{:S(2)}, u32[]{:S(2)}) collective-permute-start(bf16[16,512]{1,0:T(8,128)(2,1)S(1)} %get-tuple-element.29), channel_id=1, source_target_pairs={{0,16},{8,24},{16,0},{24,8},{1,17},{9,25},{17,1},{25,9},{2,18},{10... | collective-permute-start | bytes 49160 | tf_op jit(solution)/shard_map/ppermute | solution.py:27
  39.7 3.7 %collective-permute-start.3 = (bf16[16,512]{1,0:T(8,128)(2,1)S(1)}, bf16[16,512]{1,0:T(8,128)(2,1)S(1)}, u32[]{:S(2)}, u32[]{:S(2)}) collective-permute-start(bf16[16,512]{1,0:T(8,128)(2,1)S(1)} %get-tuple-element.29), channel_id=1, source_target_pairs={{0,8},{8,0},{16,24},{24,16},{1,9},{9,1},{17,25},{25,17},{2,10},{10... | collective-permute-start | bytes 49160 | tf_op jit(solution)/shard_map/ppermute | solution.py:27
  41.2 0.7 copy-start.18
  43.4 1.0 %copy-start.10 = (bf16[512,512]{1,0:T(8,128)(2,1)S(1)}, bf16[512,512]{1,0:T(8,128)(2,1)}, u32[]{:S(2)}) copy-start(bf16[512,512]{1,0:T(8,128)(2,1)} %refs_6_.3) | copy-start | bytes 1572868
  44.5 1.0 %copy-start.11 = (bf16[512,512]{1,0:T(8,128)(2,1)S(1)}, bf16[512,512]{1,0:T(8,128)(2,1)}, u32[]{:S(2)}) copy-start(bf16[512,512]{1,0:T(8,128)(2,1)} %refs_7_.3) | copy-start | bytes 1572868
  45.5 9.6 %copy-start.4 = (f32[2,4,256,128]{3,2,1,0:T(8,128)S(1)}, f32[2,4,256,128]{3,2,1,0:T(8,128)}, u32[]{:S(2)}) copy-start(f32[2,4,256,128]{3,2,1,0:T(8,128)} %cell_ref.3) | copy-start | bytes 3145732
  45.5 9.6 %copy-start.14 = (f32[2,4,128]{2,1,0:T(4,128)S(1)}, f32[2,4,128]{2,1,0:T(4,128)}, u32[]{:S(2)}) copy-start(f32[2,4,128]{2,1,0:T(4,128)} %norm_ref.3) | copy-start | bytes 12292
  45.5 9.6 %copy-start.16 = (f32[2,4]{1,0:T(2,128)S(1)}, f32[2,4]{1,0:T(2,128)}, u32[]{:S(2)}) copy-start(f32[2,4]{1,0:T(2,128)} %stab_ref.3) | copy-start | bytes 100
  46.1 19.3 %copy-start.5 = (bf16[1024,512]{1,0:T(8,128)(2,1)S(1)}, bf16[1024,512]{1,0:T(8,128)(2,1)}, u32[]{:S(2)}) copy-start(bf16[1024,512]{1,0:T(8,128)(2,1)} %w_ref.3) | copy-start | bytes 3145732
  65.7 3.7 %collective-permute-start.6 = (bf16[4,512]{1,0:T(4,128)(2,1)S(1)}, bf16[4,512]{1,0:T(4,128)(2,1)S(1)}, u32[]{:S(2)}, u32[]{:S(2)}) collective-permute-start(bf16[4,512]{1,0:T(4,128)(2,1)S(1)} %get-tuple-element.34), channel_id=1, source_target_pairs={{0,8},{8,0},{16,24},{24,16},{1,9},{9,1},{17,25},{25,17},{2,10},{10... | collective-permute-start | bytes 12296 | tf_op jit(solution)/shard_map/ppermute | solution.py:27
  67.2 3.6 %collective-permute-start.7 = (bf16[4,512]{1,0:T(4,128)(2,1)S(1)}, bf16[4,512]{1,0:T(4,128)(2,1)S(1)}, u32[]{:S(2)}, u32[]{:S(2)}) collective-permute-start(bf16[4,512]{1,0:T(4,128)(2,1)S(1)} %get-tuple-element.35), channel_id=1, source_target_pairs={{0,16},{8,24},{16,0},{24,8},{1,17},{9,25},{17,1},{25,9},{2,18},{10... | collective-permute-start | bytes 12296 | tf_op jit(solution)/shard_map/ppermute | solution.py:27
  67.7 4.5 %collective-permute-start.8 = (bf16[4,512]{1,0:T(4,128)(2,1)S(1)}, bf16[4,512]{1,0:T(4,128)(2,1)S(1)}, u32[]{:S(2)}, u32[]{:S(2)}) collective-permute-start(bf16[4,512]{1,0:T(4,128)(2,1)S(1)} %get-tuple-element.36), channel_id=1, source_target_pairs={{0,24},{8,16},{16,8},{24,0},{1,25},{9,17},{17,9},{25,1},{2,26},{10... | collective-permute-start | bytes 12296 | tf_op jit(solution)/shard_map/ppermute | solution.py:27

commit v3 on v2

--- a/solution.py
+++ b/solution.py
@@ -14,6 +14,7 @@
 NT = (((1,), (1,)), ((), ()))
 TN = (((0,), (0,)), ((), ()))
 MIB = 1 << 20
+PREPARE_COST = 4 * 10**9
 
 
 def pairwise(size):
@@ -61,19 +62,20 @@
 
 
 def row_blocks(ref, rows):
-    return [ref[j * rows : (j + 1) * rows, :] for j in range(ref.shape[0] // rows)]
+    whole = ref[...].astype(F32)
+    return [whole[j * rows : (j + 1) * rows, :] for j in range(ref.shape[0] // rows)]
 
 
 def project(x, gain_ref, weights, small_ref, payload_ref, y_ref, narrow):
     batch = x.shape[0]
     squares = jnp.sum(x * x, axis=1, keepdims=True)
-    scaled = (x * gain_ref[...].astype(F32)).astype(BF16)
+    scaled = (x * gain_ref[...]).astype(BF16)
     at = 0
     for w_ref in weights:
         width = w_ref.shape[1]
         y_ref[:, at : at + width] = jnp.dot(scaled, w_ref[...], preferred_element_type=F32)
         at += width
-    gates = lax.dot_general(scaled, small_ref[...], NT, preferred_element_type=F32)
+    gates = lax.dot_general(scaled, small_ref[...].astype(BF16), NT, preferred_element_type=F32)
     lane = lax.broadcasted_iota(jnp.int32, (batch, LANES), 1)
     gates = jnp.where(lane == narrow, squares, gates)
     high = gates.astype(BF16).astype(F32)
@@ -110,9 +112,9 @@
     project(x, gain_ref, (wq, wk, wv, wo), small_ref, payload_ref, y_ref, narrow)
 
 
-def state_body(
+def read_body(
     width, received_ref, cell_ref, norm_ref, stab_ref,
-    gated_ref, cell_out, norm_out, stab_out, read_ref,
+    gated_ref, stab_out, gates_out, keys_out, values_out, read_ref,
 ):
     seqs, heads, dhv, dhk = cell_ref.shape
     nk, nv = heads * dhk, heads * dhv
@@ -131,45 +133,60 @@
     stab_out[...] = stab_next
     retain = jnp.exp(kept - stab_next)
     admitted = jnp.exp(input_pre - stab_next)
+    gates_out[0] = retain
+    gates_out[1] = admitted
     queries = total[:, :nk] * (scale * dhk ** (-0.5))
     keys = total[:, nk : 2 * nk] * scale
     values = total[:, 2 * nk : 2 * nk + nv] * scale
+    keys_out[...] = keys
+    values_out[...] = values
     gate = jax.nn.sigmoid(total[:, 2 * nk + nv : base] * scale)
+    row = lax.broadcasted_iota(jnp.int32, (8, dhk), 0)
+    for s in range(seqs):
+        for h in range(heads):
+            keep = retain[s : s + 1, h : h + 1]
+            admit = admitted[s : s + 1, h : h + 1]
+            query = queries[s : s + 1, h * dhk : (h + 1) * dhk]
+            key = keys[s : s + 1, h * dhk : (h + 1) * dhk]
+            value = values[s : s + 1, h * dhv : (h + 1) * dhv]
+            matched = jnp.sum(key * query, axis=1, keepdims=True)
+            stored = jnp.sum(norm_ref[s, h : h + 1, :] * query, axis=1, keepdims=True)
+            bound = jnp.maximum(jnp.abs(keep * stored + admit * matched), 1.0)
+            query_high = query.astype(BF16).astype(F32)
+            asks = jnp.where(row == 0, query_high, jnp.where(row == 1, query - query_high, 0.0))
+            asks = asks.astype(BF16)
+            cell = cell_ref[s, h]
+            cell_high = cell.astype(BF16)
+            read = lax.dot_general(asks, cell_high, NT, preferred_element_type=F32)
+            low = (cell - cell_high.astype(F32)).astype(BF16)
+            read = read + lax.dot_general(asks, low, NT, preferred_element_type=F32)
+            numerator = keep * jnp.sum(read, axis=0, keepdims=True) + (admit * matched) * value
+            read_ref[s : s + 1, h * dhv : (h + 1) * dhv] = numerator / bound
+    gated = (read_ref[...] * gate).astype(BF16)
+    for d in range(gated_ref.shape[0]):
+        gated_ref[d] = gated
+
+
+def store_body(cell_ref, norm_ref, gates_ref, keys_ref, values_ref, cell_out, norm_out):
+    seqs, heads, dhv, dhk = cell_ref.shape
+    retain, admitted = gates_ref[0], gates_ref[1]
     row = lax.broadcasted_iota(jnp.int32, (8, dhk), 0)
     row_v = lax.broadcasted_iota(jnp.int32, (8, dhv), 0)
     for s in range(seqs):
         for h in range(heads):
             keep = retain[s : s + 1, h : h + 1]
             admit = admitted[s : s + 1, h : h + 1]
-            query = queries[s : s + 1, h * dhk : (h + 1) * dhk]
-            key = keys[s : s + 1, h * dhk : (h + 1) * dhk]
-            value = values[s : s + 1, h * dhv : (h + 1) * dhv] * admit
-            norm_next = keep * norm_ref[s, h : h + 1, :] + admit * key
-            norm_out[s, h : h + 1, :] = norm_next
-            bound = jnp.maximum(jnp.abs(jnp.sum(norm_next * query, axis=1, keepdims=True)), 1.0)
+            key = keys_ref[s : s + 1, h * dhk : (h + 1) * dhk]
+            value = values_ref[s : s + 1, h * dhv : (h + 1) * dhv] * admit
+            norm_out[s, h : h + 1, :] = keep * norm_ref[s, h : h + 1, :] + admit * key
             key_high = key.astype(BF16).astype(F32)
-            key_low = key - key_high
             value_high = value.astype(BF16).astype(F32)
-            value_low = value - value_high
-            left = jnp.where(row_v < 2, value_high, jnp.where(row_v < 4, value_low, 0.0))
-            right = jnp.where(row & 1 == 0, key_high, key_low)
+            left = jnp.where(row_v < 2, value_high, jnp.where(row_v < 4, value - value_high, 0.0))
+            right = jnp.where(row & 1 == 0, key_high, key - key_high)
             outer = lax.dot_general(
                 left.astype(BF16), right.astype(BF16), TN, preferred_element_type=F32
             )
-            cell_next = keep * cell_ref[s, h] + outer
-            cell_out[s, h] = cell_next
-            query_high = query.astype(BF16).astype(F32)
-            asks = jnp.where(row == 0, query_high, jnp.where(row == 1, query - query_high, 0.0))
-            asks = asks.astype(BF16)
-            cell_high = cell_next.astype(BF16)
-            read = lax.dot_general(asks, cell_high, NT, preferred_element_type=F32)
-            low = (cell_next - cell_high.astype(F32)).astype(BF16)
-            read = read + lax.dot_general(asks, low, NT, preferred_element_type=F32)
-            numerator = jnp.sum(read, axis=0, keepdims=True)
-            read_ref[s : s + 1, h * dhv : (h + 1) * dhv] = numerator / bound
-    gated = (read_ref[...] * gate).astype(BF16)
-    for d in range(gated_ref.shape[0]):
-        gated_ref[d] = gated
+            cell_out[s, h] = keep * cell_ref[s, h] + outer
 
 
 def mix(gathered_ref, w_ref, x_ref):
@@ -213,12 +230,23 @@
     hidden_ref[...] = total.astype(BF16)
 
 
-def own_gates(w_input, w_forget, heads):
-    offset = lax.axis_index("tp") * heads
-    rows = jnp.concatenate(
-        [lax.dynamic_slice_in_dim(w.T, offset, heads, 0) for w in (w_input, w_forget)], axis=0
-    )
-    return jnp.pad(rows, ((0, LANES - rows.shape[0]), (0, 0)))
+def open_body(ref):
+    ref[...] = jnp.zeros_like(ref)
+
+
+def prepare_body(heads, *refs):
+    refs = refs[1:]
+    count = len(refs) // 5
+    ins, outs = refs[: 3 * count], refs[3 * count :]
+    me = lax.axis_index("tp")
+    for c in range(count):
+        gain_ref, input_ref, forget_ref = ins[3 * c : 3 * c + 3]
+        gain_out, small_ref = outs[2 * c : 2 * c + 2]
+        gain_out[...] = gain_ref[...].astype(F32)[None, :]
+        rows = [pick(row_blocks(w, heads), me) for w in (input_ref, forget_ref)]
+        small_ref[...] = jnp.zeros_like(small_ref)
+        for j, block in enumerate(rows):
+            small_ref[j * heads : (j + 1) * heads, :] = block.astype(F32)
 
 
 def per_device(sizes, tokens, *args):
@@ -233,8 +261,21 @@
     payload = jax.ShapeDtypeStruct((dp, seqs, payload_width), BF16)
     stream = jax.ShapeDtypeStruct((batch, features), F32)
     gated = jax.ShapeDtypeStruct((dp, seqs, nv), BF16)
-    small = [own_gates(cell[5], cell[6], heads) for cell in cells]
-    gains = [cell[0].reshape(1, features) for cell in cells]
+    opened = call(open_body, [jax.ShapeDtypeStruct((8, LANES), F32)], [], PREPARE_COST, MIB)
+    prepared = call(
+        functools.partial(prepare_body, heads),
+        [
+            jax.ShapeDtypeStruct((1, features), F32),
+            jax.ShapeDtypeStruct((LANES, features), F32),
+        ]
+        * 2,
+        [],
+        PREPARE_COST,
+        4 * MIB,
+        *opened,
+        *(x for cell in cells for x in (cell[0], cell[5].T, cell[6].T)),
+    )
+    gains, small = prepared[0::2], prepared[1::2]
     project_scratch = [pltpu.VMEM((batch, payload_width), F32)]
     project_cost = 2 * batch * features * payload_width
     mix_scratch = pltpu.VMEM((batch, nv), F32)
@@ -244,21 +285,37 @@
     def exchange_dp(x):
         return lax.all_to_all(x, "dp", 0, 0)
 
-    def update(received, cell):
-        return call(
-            functools.partial(state_body, features * dp),
+    def read(received, cell):
+        gated_rows, stab, gates, keys, values = call(
+            functools.partial(read_body, features * dp),
             [
                 gated,
-                jax.ShapeDtypeStruct(cell[8].shape, F32),
-                jax.ShapeDtypeStruct(cell[9].shape, F32),
                 jax.ShapeDtypeStruct(cell[10].shape, F32),
+                jax.ShapeDtypeStruct((2, *cell[10].shape), F32),
+                jax.ShapeDtypeStruct((seqs, nk), F32),
+                jax.ShapeDtypeStruct((seqs, nv), F32),
             ],
             [pltpu.VMEM((seqs, nv), F32)],
             state_cost,
-            12 * MIB,
+            8 * MIB,
             received,
             *cell[8:],
         )
+        cell_next, norm_next = call(
+            store_body,
+            [
+                jax.ShapeDtypeStruct(cell[8].shape, F32),
+                jax.ShapeDtypeStruct(cell[9].shape, F32),
+            ],
+            [],
+            state_cost,
+            8 * MIB,
+            *cell[8:10],
+            gates,
+            keys,
+            values,
+        )
+        return gated_rows, cell_next, norm_next, stab
 
     if paired:
         pieces = [tokens] + peers([tokens] * (tp - 1), "tp", tp)
@@ -276,7 +333,7 @@
         *cells[0][1:5],
         small[0],
     )
-    shared, *first = update(exchange_dp(sums), cells[0])
+    shared, *first = read(exchange_dp(sums), cells[0])
     sent, own = call(
         middle_body,
         [jax.ShapeDtypeStruct((batch, features), BF16), stream],
@@ -291,6 +348,7 @@
     else:
         own = jnp.zeros_like(own)
         pieces = [lax.all_to_all(jnp.broadcast_to(sent[None], (tp, batch, features)), "tp", 0, 0)]
+    pieces, first = lax.optimization_barrier((pieces, first))
     sums, x = call(
         functools.partial(second_body, len(pieces), 2 * heads),
         [payload, stream],
@@ -304,7 +362,7 @@
         *cells[1][1:5],
         small[1],
     )
-    shared, *second = update(exchange_dp(sums), cells[1])
+    shared, *second = read(exchange_dp(sums), cells[1])
     block = jax.ShapeDtypeStruct((rows, features), BF16)
     if paired:
         outs = [jax.ShapeDtypeStruct((rows, features), F32)] + [block] * (tp - 1)

time: 73.6 us -> 63.3 us (0.86)
  local copies, waits for them, and re-layouts: 9.44 us -> 0.76 us
  blocking collectives: 28.1 us -> 36.4 us
  waiting for transfers between devices: 12.8 us -> 6.24 us
  starting transfers between devices: 15 us -> 11.7 us
    all_to_all x3 -> x4, blocking collectives: 28.1 us -> 36.4 us  [exchange_dp(): return lax.all_to_all(x, 'dp', 0, 0)]
    unnamed x38 -> x46, local copies, waits for them, and re-layouts: 7.98 us -> 0.76 us
    all_to_all x1 -> x0, waiting for transfers between devices: 4.94 us -> none  [exchange_dp(): return lax.all_to_all(x, 'dp', 0, 0)]
    all_to_all x1 -> x0, starting transfers between devices: 3.34 us -> none  [exchange_dp(): return lax.all_to_all(x, 'dp', 0, 0)]
    ppermute x9, waiting for transfers between devices: 7.84 us -> 6.24 us  [peers(): lax.ppermute(pieces[k - 1], axis, [(i, i ^ k) for i in range(size)])]
    dynamic_slice x2 -> x0, local copies, waits for them, and re-layouts: 1.45 us -> none  [own_gates(): lax.dynamic_slice_in_dim(w.T, offset, heads, 0)]
    pallas_call x7 -> x11, Pallas kernels: 6.73 us -> 7.09 us  [call(): pl.pallas_call(body, out_shape=outs, in_specs=[pl.BlockSpec(memory_space=...]
  transfers between devices with their start and end apart: 10 -> 9, of which waited for: 8 -> 5; matrix products, arithmetic and copies ran while one was open for 2% -> 0% of each run, Pallas kernels for 0% -> 5%
where the time goes in v3:
time: 63.3 us; the launch traced here: 63 us
  blocking collectives  36.4 us (58%)
  starting transfers between devices  11.7 us (18%)
  Pallas kernels  7.09 us (11%)
  waiting for transfers between devices  6.24 us (10%)
  between operations  0.87 us (1%)
  local copies, waits for them, and re-layouts  0.76 us (1%)
    all_to_all x4, blocking collectives, exchange_dp(): return lax.all_to_all(x, 'dp', 0, 0)  36.4 us
    ppermute x9, starting transfers between devices, peers(): lax.ppermute(pieces[k - 1], axis, [(i, i ^ k) for i in range(size)])  11.7 us
    pallas_call x11, Pallas kernels, call(): pl.pallas_call(body, out_shape=outs, in_specs=[pl.BlockSpec(memory_space=...  7.09 us
    ppermute x9, waiting for transfers between devices, peers(): lax.ppermute(pieces[k - 1], axis, [(i, i ^ k) for i in range(size)])  6.24 us
  transfers between devices with their start and end apart: 9, of which 5 were waited for; matrix products, arithmetic and copies ran while one was open for 0% of the time, Pallas kernels for 5%

profile of v3, /device:TPU:0, one launch (start us, length us, event | category | flops | bytes accessed | tf_op | source)
XLA Modules:
  0.0 63.0 jit_solution(15329657785203142560)
XLA Ops:
  0.6 0.0 copy-start.20
  0.6 0.0 copy-start.19
  0.7 0.0 copy-start.18
  0.7 3.1 %collective-permute-start.1 = (bf16[4,512]{1,0:T(4,128)(2,1)}, bf16[4,512]{1,0:T(4,128)(2,1)S(1)}, u32[]{:S(2)}, u32[]{:S(2)}) collective-permute-start(bf16[4,512]{1,0:T(4,128)(2,1)} %refs_0_.1), channel_id=1, source_target_pairs={{0,16},{8,24},{16,0},{24,8},{1,17},{9,25},{17,1},{25,9},{2,18},{10... | collective-permute-start | bytes 12296 | tf_op jit(solution)/shard_map/ppermute | solution.py:28
  3.7 1.5 %collective-permute-start = (bf16[4,512]{1,0:T(4,128)(2,1)}, bf16[4,512]{1,0:T(4,128)(2,1)S(1)}, u32[]{:S(2)}, u32[]{:S(2)}) collective-permute-start(bf16[4,512]{1,0:T(4,128)(2,1)} %refs_0_.1), channel_id=1, source_target_pairs={{0,8},{8,0},{16,24},{24,16},{1,9},{9,1},{17,25},{25,17},{2,10},{10... | collective-permute-start | bytes 12296 | tf_op jit(solution)/shard_map/ppermute | solution.py:28
  5.2 0.1 collective-permute-start.2
  5.3 0.6 %copy-done.22 = bf16[512]{0:T(512)(128)(2,1)S(1)} copy-done((bf16[512]{0:T(512)(128)(2,1)S(1)}, bf16[512]{0:T(512)(128)(2,1)}, u32[]{:S(2)}) %copy-start.22) | copy-done | bytes 1048
  6.0 0.0 copy-done.21
  6.0 0.0 copy-start.14
  6.0 0.1 shard_map.271
  6.1 0.0 collective-permute-done.1.refs_2_
  6.1 1.5 %collective-permute-done.refs_1_ = bf16[4,512]{1,0:T(4,128)(2,1)S(1)} collective-permute-done((bf16[4,512]{1,0:T(4,128)(2,1)}, bf16[4,512]{1,0:T(4,128)(2,1)S(1)}, u32[]{:S(2)}, u32[]{:S(2)}) %collective-permute-start) | collective-permute-done | bytes 4128 | tf_op jit(solution)/shard_map/ppermute | solution.py:28
  7.6 2.4 %collective-permute-done.2.refs_3_ = bf16[4,512]{1,0:T(4,128)(2,1)S(1)} collective-permute-done((bf16[4,512]{1,0:T(4,128)(2,1)}, bf16[4,512]{1,0:T(4,128)(2,1)S(1)}, u32[]{:S(2)}, u32[]{:S(2)}) %collective-permute-start.2) | collective-permute-done | bytes 4128 | tf_op jit(solution)/shard_map/ppermute | solution.py:28
  10.0 0.0 copy-start
  10.0 0.0 copy-start.12
  10.0 0.0 copy-start.15
  10.0 0.0 copy-start.10
  10.0 0.0 copy-start.11
  10.0 0.6 shard_map.272
  10.6 0.0 copy-start.6
  10.6 11.2 %all_to_all.20.received_ref = bf16[8,2,3328]{2,1,0:T(2,128)(2,1)S(1)} all-to-all(bf16[8,2,3328]{2,1,0:T(2,128)(2,1)S(1)} %get-tuple-element.44), channel_id=1, replica_groups=mesh['tp'=4,'dp'=8] {'dp'}, dimensions={0} | all-to-all | bytes 212992 | tf_op jit(solution)/shard_map/all_to_all | solution.py:286
  21.9 0.9 %shard_map.273 = (bf16[8,2,1024]{2,1,0:T(2,128)(2,1)S(1)}, f32[2,4]{1,0:T(2,128)}, f32[2,2,4]{2,1,0:T(2,128)S(1)}, f32[2,512]{1,0:T(2,128)S(1)}, f32[2,1024]{1,0:T(2,128)S(1)}) custom-call(bf16[8,2,3328]{2,1,0:T(2,128)(2,1)S(1)} %all_to_all.20.received_ref, f32[2,4,256,128]{3,2,1,0:T(8,128)S(1)} %copy-done, f32[2,4,128]{2,1,0:T(4,128)S(1)} %copy-done.12, ...), custom_call_target="tpu_custom_call" | custom-call | flops 4194304 | bytes 262144 | tf_op jit(solution)/shard_map/pallas_call | solution.py:38
  22.8 8.1 %all_to_all.21.gathered_ref = bf16[8,2,1024]{2,1,0:T(2,128)(2,1)S(1)} all-to-all(bf16[8,2,1024]{2,1,0:T(2,128)(2,1)S(1)} %get-tuple-element.45), channel_id=1, replica_groups=mesh['tp'=4,'dp'=8] {'dp'}, dimensions={0} | all-to-all | bytes 65536 | tf_op jit(solution)/shard_map/all_to_all | solution.py:286
  30.9 0.2 shard_map.274
  31.1 0.7 %collective-permute-start.5 = (bf16[16,512]{1,0:T(8,128)(2,1)S(1)}, bf16[16,512]{1,0:T(8,128)(2,1)S(1)}, u32[]{:S(2)}, u32[]{:S(2)}) collective-permute-start(bf16[16,512]{1,0:T(8,128)(2,1)S(1)} %get-tuple-element.47), channel_id=1, source_target_pairs={{0,24},{8,16},{16,8},{24,0},{1,25},{9,17},{17,9},{25,1},{2,26},{10... | collective-permute-start | bytes 49160 | tf_op jit(solution)/shard_map/ppermute | solution.py:28
  31.8 1.3 %collective-permute-start.4 = (bf16[16,512]{1,0:T(8,128)(2,1)S(1)}, bf16[16,512]{1,0:T(8,128)(2,1)S(1)}, u32[]{:S(2)}, u32[]{:S(2)}) collective-permute-start(bf16[16,512]{1,0:T(8,128)(2,1)S(1)} %get-tuple-element.47), channel_id=1, source_target_pairs={{0,16},{8,24},{16,0},{24,8},{1,17},{9,25},{17,1},{25,9},{2,18},{10... | collective-permute-start | bytes 49160 | tf_op jit(solution)/shard_map/ppermute | solution.py:28
  33.2 1.5 %collective-permute-start.3 = (bf16[16,512]{1,0:T(8,128)(2,1)S(1)}, bf16[16,512]{1,0:T(8,128)(2,1)S(1)}, u32[]{:S(2)}, u32[]{:S(2)}) collective-permute-start(bf16[16,512]{1,0:T(8,128)(2,1)S(1)} %get-tuple-element.47), channel_id=1, source_target_pairs={{0,8},{8,0},{16,24},{24,16},{1,9},{9,1},{17,25},{25,17},{2,10},{10... | collective-permute-start | bytes 49160 | tf_op jit(solution)/shard_map/ppermute | solution.py:28
  34.7 1.4 %shard_map.275 = (f32[2,4,256,128]{3,2,1,0:T(8,128)}, f32[2,4,128]{2,1,0:T(4,128)}) custom-call(f32[2,4,256,128]{3,2,1,0:T(8,128)S(1)} %copy-done, f32[2,4,128]{2,1,0:T(4,128)S(1)} %copy-done.12, f32[2,2,4]{2,1,0:T(2,128)S(1)} %get-tuple-element.48.gates_ref, f32[2,512]{1,0:T(2,128)S(1)} %get-tuple-element.49.keys_ref, ...), custom_call_target="tpu_custom_call" | custom-call | flops 4194304 | bytes 262144 | tf_op jit(solution)/shard_map/pallas_call | solution.py:38
  36.1 0.0 collective-permute-done.5.refs_4_
  36.1 0.0 collective-permute-done.4.refs_3_
  36.1 0.8 %collective-permute-done.3.refs_2_ = bf16[16,512]{1,0:T(8,128)(2,1)S(1)} collective-permute-done((bf16[16,512]{1,0:T(8,128)(2,1)S(1)}, bf16[16,512]{1,0:T(8,128)(2,1)S(1)}, u32[]{:S(2)}, u32[]{:S(2)}) %collective-permute-start.3) | collective-permute-done | bytes 16416 | tf_op jit(solution)/shard_map/ppermute | solution.py:28
  36.9 0.0 copy-start.1
  36.9 0.0 copy-start.13
  36.9 0.0 copy-start.16
  37.0 0.6 shard_map.276
  37.6 0.0 copy-start.7
  37.6 8.9 %all_to_all.22.received_ref = bf16[8,2,3328]{2,1,0:T(2,128)(2,1)S(1)} all-to-all(bf16[8,2,3328]{2,1,0:T(2,128)(2,1)S(1)} %get-tuple-element.60), channel_id=1, replica_groups=mesh['tp'=4,'dp'=8] {'dp'}, dimensions={0} | all-to-all | bytes 212992 | tf_op jit(solution)/shard_map/all_to_all | solution.py:286
  46.5 0.9 %shard_map.277 = (bf16[8,2,1024]{2,1,0:T(2,128)(2,1)S(1)}, f32[2,4]{1,0:T(2,128)}, f32[2,2,4]{2,1,0:T(2,128)S(1)}, f32[2,512]{1,0:T(2,128)S(1)}, f32[2,1024]{1,0:T(2,128)S(1)}) custom-call(bf16[8,2,3328]{2,1,0:T(2,128)(2,1)S(1)} %all_to_all.22.received_ref, f32[2,4,256,128]{3,2,1,0:T(8,128)S(1)} %copy-done.1, f32[2,4,128]{2,1,0:T(4,128)S(1)} %copy-done.13, ...), custom_call_target="tpu_custom_call" | custom-call | flops 4194304 | bytes 262144 | tf_op jit(solution)/shard_map/pallas_call | solution.py:38
  47.4 8.1 %all_to_all.23.gathered_ref = bf16[8,2,1024]{2,1,0:T(2,128)(2,1)S(1)} all-to-all(bf16[8,2,1024]{2,1,0:T(2,128)(2,1)S(1)} %get-tuple-element.61), channel_id=1, replica_groups=mesh['tp'=4,'dp'=8] {'dp'}, dimensions={0} | all-to-all | bytes 65536 | tf_op jit(solution)/shard_map/all_to_all | solution.py:286
  55.5 0.3 shard_map.278
  55.8 1.6 %collective-permute-start.6 = (bf16[4,512]{1,0:T(4,128)(2,1)S(1)}, bf16[4,512]{1,0:T(4,128)(2,1)S(1)}, u32[]{:S(2)}, u32[]{:S(2)}) collective-permute-start(bf16[4,512]{1,0:T(4,128)(2,1)S(1)} %get-tuple-element.63), channel_id=1, source_target_pairs={{0,8},{8,0},{16,24},{24,16},{1,9},{9,1},{17,25},{25,17},{2,10},{10... | collective-permute-start | bytes 12296 | tf_op jit(solution)/shard_map/ppermute | solution.py:28
  57.4 0.5 collective-permute-start.7
  57.9 1.5 %collective-permute-start.8 = (bf16[4,512]{1,0:T(4,128)(2,1)S(1)}, bf16[4,512]{1,0:T(4,128)(2,1)S(1)}, u32[]{:S(2)}, u32[]{:S(2)}) collective-permute-start(bf16[4,512]{1,0:T(4,128)(2,1)S(1)} %get-tuple-element.65), channel_id=1, source_target_pairs={{0,24},{8,16},{16,8},{24,0},{1,25},{9,17},{17,9},{25,1},{2,26},{10... | collective-permute-start | bytes 12296 | tf_op jit(solution)/shard_map/ppermute | solution.py:28
  59.4 1.4 %shard_map.280 = (f32[2,4,256,128]{3,2,1,0:T(8,128)}, f32[2,4,128]{2,1,0:T(4,128)}) custom-call(f32[2,4,256,128]{3,2,1,0:T(8,128)S(1)} %copy-done.1, f32[2,4,128]{2,1,0:T(4,128)S(1)} %copy-done.13, f32[2,2,4]{2,1,0:T(2,128)S(1)} %get-tuple-element.69.gates_ref, f32[2,512]{1,0:T(2,128)S(1)} %get-tuple-element.70.keys_ref, ...), custom_call_target="tpu_custom_call" | custom-call | flops 4194304 | bytes 262144 | tf_op jit(solution)/shard_map/pallas_call | solution.py:38
  60.8 0.0 collective-permute-done.6.refs_1_
  60.8 0.2 collective-permute-done.7.refs_2_
  61.0 1.4 %collective-permute-done.8.refs_3_ = bf16[4,512]{1,0:T(4,128)(2,1)S(1)} collective-permute-done((bf16[4,512]{1,0:T(4,128)(2,1)S(1)}, bf16[4,512]{1,0:T(4,128)(2,1)S(1)}, u32[]{:S(2)}, u32[]{:S(2)}) %collective-permute-start.8) | collective-permute-done | bytes 4128 | tf_op jit(solution)/shard_map/ppermute | solution.py:28
  62.4 0.6 shard_map.279
  (31 shorter events, 0.1 us)
Async XLA Ops:
  0.6 4.7 %copy-start.20 = (bf16[512,16]{0,1:T(8,128)(2,1)S(1)}, bf16[512,16]{0,1:T(8,128)(2,1)}, u32[]{:S(2)}) copy-start(bf16[512,16]{0,1:T(8,128)(2,1)} %param.41) | copy-start | bytes 49156
  0.6 4.6 %copy-start.19 = (bf16[512,16]{0,1:T(8,128)(2,1)S(1)}, bf16[512,16]{0,1:T(8,128)(2,1)}, u32[]{:S(2)}) copy-start(bf16[512,16]{0,1:T(8,128)(2,1)} %param.40) | copy-start | bytes 49156
  0.7 4.6 %copy-start.18 = (bf16[512,16]{0,1:T(8,128)(2,1)S(1)}, bf16[512,16]{0,1:T(8,128)(2,1)}, u32[]{:S(2)}) copy-start(bf16[512,16]{0,1:T(8,128)(2,1)} %param.30) | copy-start | bytes 49156
  0.7 4.6 %copy-start.17 = (bf16[512,16]{0,1:T(8,128)(2,1)S(1)}, bf16[512,16]{0,1:T(8,128)(2,1)}, u32[]{:S(2)}) copy-start(bf16[512,16]{0,1:T(8,128)(2,1)} %param.29) | copy-start | bytes 49156
  0.7 5.4 %collective-permute-start.1 = (bf16[4,512]{1,0:T(4,128)(2,1)}, bf16[4,512]{1,0:T(4,128)(2,1)S(1)}, u32[]{:S(2)}, u32[]{:S(2)}) collective-permute-start(bf16[4,512]{1,0:T(4,128)(2,1)} %refs_0_.1), channel_id=1, source_target_pairs={{0,16},{8,24},{16,0},{24,8},{1,17},{9,25},{17,1},{25,9},{2,18},{10... | collective-permute-start | bytes 12296 | tf_op jit(solution)/shard_map/ppermute | solution.py:28
  3.7 3.8 %collective-permute-start = (bf16[4,512]{1,0:T(4,128)(2,1)}, bf16[4,512]{1,0:T(4,128)(2,1)S(1)}, u32[]{:S(2)}, u32[]{:S(2)}) collective-permute-start(bf16[4,512]{1,0:T(4,128)(2,1)} %refs_0_.1), channel_id=1, source_target_pairs={{0,8},{8,0},{16,24},{24,16},{1,9},{9,1},{17,25},{25,17},{2,10},{10... | collective-permute-start | bytes 12296 | tf_op jit(solution)/shard_map/ppermute | solution.py:28
  5.2 4.7 %collective-permute-start.2 = (bf16[4,512]{1,0:T(4,128)(2,1)}, bf16[4,512]{1,0:T(4,128)(2,1)S(1)}, u32[]{:S(2)}, u32[]{:S(2)}) collective-permute-start(bf16[4,512]{1,0:T(4,128)(2,1)} %refs_0_.1), channel_id=1, source_target_pairs={{0,24},{8,16},{16,8},{24,0},{1,25},{9,17},{17,9},{25,1},{2,26},{10... | collective-permute-start | bytes 12296 | tf_op jit(solution)/shard_map/ppermute | solution.py:28
  5.3 0.7 %copy-start.22 = (bf16[512]{0:T(512)(128)(2,1)S(1)}, bf16[512]{0:T(512)(128)(2,1)}, u32[]{:S(2)}) copy-start(bf16[512]{0:T(512)(128)(2,1)} %refs_4_.1) | copy-start | bytes 3076
  5.3 0.7 %copy-start.21 = (bf16[512]{0:T(512)(128)(2,1)S(1)}, bf16[512]{0:T(512)(128)(2,1)}, u32[]{:S(2)}) copy-start(bf16[512]{0:T(512)(128)(2,1)} %refs_1_.1) | copy-start | bytes 3076
  6.0 4.0 %copy-start.2 = (bf16[512,1024]{1,0:T(8,128)(2,1)S(1)}, bf16[512,1024]{1,0:T(8,128)(2,1)}, u32[]{:S(2)}) copy-start(bf16[512,1024]{1,0:T(8,128)(2,1)} %refs_7_.2) | copy-start | bytes 3145732
  6.0 4.0 %copy-start.3 = (bf16[512,1024]{1,0:T(8,128)(2,1)S(1)}, bf16[512,1024]{1,0:T(8,128)(2,1)}, u32[]{:S(2)}) copy-start(bf16[512,1024]{1,0:T(8,128)(2,1)} %refs_8_.2) | copy-start | bytes 3145732
  6.0 4.0 %copy-start.8 = (bf16[512,512]{1,0:T(8,128)(2,1)S(1)}, bf16[512,512]{1,0:T(8,128)(2,1)}, u32[]{:S(2)}) copy-start(bf16[512,512]{1,0:T(8,128)(2,1)} %refs_5_.1) | copy-start | bytes 1572868
  6.0 4.0 %copy-start.9 = (bf16[512,512]{1,0:T(8,128)(2,1)S(1)}, bf16[512,512]{1,0:T(8,128)(2,1)}, u32[]{:S(2)}) copy-start(bf16[512,512]{1,0:T(8,128)(2,1)} %refs_6_.2) | copy-start | bytes 1572868
  6.0 4.0 %copy-start.14 = (bf16[4,512]{1,0:T(4,128)(2,1)S(1)}, bf16[4,512]{1,0:T(4,128)(2,1)}, u32[]{:S(2)}) copy-start(bf16[4,512]{1,0:T(4,128)(2,1)} %refs_0_.1) | copy-start | bytes 12292
  10.0 11.9 %copy-start = (f32[2,4,256,128]{3,2,1,0:T(8,128)S(1)}, f32[2,4,256,128]{3,2,1,0:T(8,128)}, u32[]{:S(2)}) copy-start(f32[2,4,256,128]{3,2,1,0:T(8,128)} %cell_ref.5) | copy-start | bytes 3145732
  10.0 11.9 %copy-start.12 = (f32[2,4,128]{2,1,0:T(4,128)S(1)}, f32[2,4,128]{2,1,0:T(4,128)}, u32[]{:S(2)}) copy-start(f32[2,4,128]{2,1,0:T(4,128)} %norm_ref.5) | copy-start | bytes 12292
  10.0 11.9 %copy-start.15 = (f32[2,4]{1,0:T(2,128)S(1)}, f32[2,4]{1,0:T(2,128)}, u32[]{:S(2)}) copy-start(f32[2,4]{1,0:T(2,128)} %stab_ref.2) | copy-start | bytes 100
  10.0 26.9 %copy-start.10 = (bf16[512,512]{1,0:T(8,128)(2,1)S(1)}, bf16[512,512]{1,0:T(8,128)(2,1)}, u32[]{:S(2)}) copy-start(bf16[512,512]{1,0:T(8,128)(2,1)} %refs_6_.3) | copy-start | bytes 1572868
  10.0 26.9 %copy-start.11 = (bf16[512,512]{1,0:T(8,128)(2,1)S(1)}, bf16[512,512]{1,0:T(8,128)(2,1)}, u32[]{:S(2)}) copy-start(bf16[512,512]{1,0:T(8,128)(2,1)} %refs_7_.3) | copy-start | bytes 1572868
  10.6 20.3 %copy-start.6 = (bf16[1024,512]{1,0:T(8,128)(2,1)S(1)}, bf16[1024,512]{1,0:T(8,128)(2,1)}, u32[]{:S(2)}) copy-start(bf16[1024,512]{1,0:T(8,128)(2,1)} %w_ref.2) | copy-start | bytes 3145732
  30.9 6.0 %copy-start.4 = (bf16[512,1024]{1,0:T(8,128)(2,1)S(1)}, bf16[512,1024]{1,0:T(8,128)(2,1)}, u32[]{:S(2)}) copy-start(bf16[512,1024]{1,0:T(8,128)(2,1)} %refs_8_.3) | copy-start | bytes 3145732
  30.9 6.0 %copy-start.5 = (bf16[512,1024]{1,0:T(8,128)(2,1)S(1)}, bf16[512,1024]{1,0:T(8,128)(2,1)}, u32[]{:S(2)}) copy-start(bf16[512,1024]{1,0:T(8,128)(2,1)} %refs_9_.1) | copy-start | bytes 3145732
  31.1 5.0 %collective-permute-start.5 = (bf16[16,512]{1,0:T(8,128)(2,1)S(1)}, bf16[16,512]{1,0:T(8,128)(2,1)S(1)}, u32[]{:S(2)}, u32[]{:S(2)}) collective-permute-start(bf16[16,512]{1,0:T(8,128)(2,1)S(1)} %get-tuple-element.47), channel_id=1, source_target_pairs={{0,24},{8,16},{16,8},{24,0},{1,25},{9,17},{17,9},{25,1},{2,26},{10... | collective-permute-start | bytes 49160 | tf_op jit(solution)/shard_map/ppermute | solution.py:28
  31.8 4.3 %collective-permute-start.4 = (bf16[16,512]{1,0:T(8,128)(2,1)S(1)}, bf16[16,512]{1,0:T(8,128)(2,1)S(1)}, u32[]{:S(2)}, u32[]{:S(2)}) collective-permute-start(bf16[16,512]{1,0:T(8,128)(2,1)S(1)} %get-tuple-element.47), channel_id=1, source_target_pairs={{0,16},{8,24},{16,0},{24,8},{1,17},{9,25},{17,1},{25,9},{2,18},{10... | collective-permute-start | bytes 49160 | tf_op jit(solution)/shard_map/ppermute | solution.py:28
  33.2 3.7 %collective-permute-start.3 = (bf16[16,512]{1,0:T(8,128)(2,1)S(1)}, bf16[16,512]{1,0:T(8,128)(2,1)S(1)}, u32[]{:S(2)}, u32[]{:S(2)}) collective-permute-start(bf16[16,512]{1,0:T(8,128)(2,1)S(1)} %get-tuple-element.47), channel_id=1, source_target_pairs={{0,8},{8,0},{16,24},{24,16},{1,9},{9,1},{17,25},{25,17},{2,10},{10... | collective-permute-start | bytes 49160 | tf_op jit(solution)/shard_map/ppermute | solution.py:28
  36.9 9.6 %copy-start.1 = (f32[2,4,256,128]{3,2,1,0:T(8,128)S(1)}, f32[2,4,256,128]{3,2,1,0:T(8,128)}, u32[]{:S(2)}) copy-start(f32[2,4,256,128]{3,2,1,0:T(8,128)} %cell_ref.7) | copy-start | bytes 3145732
  36.9 9.6 %copy-start.13 = (f32[2,4,128]{2,1,0:T(4,128)S(1)}, f32[2,4,128]{2,1,0:T(4,128)}, u32[]{:S(2)}) copy-start(f32[2,4,128]{2,1,0:T(4,128)} %norm_ref.7) | copy-start | bytes 12292
  36.9 9.6 %copy-start.16 = (f32[2,4]{1,0:T(2,128)S(1)}, f32[2,4]{1,0:T(2,128)}, u32[]{:S(2)}) copy-start(f32[2,4]{1,0:T(2,128)} %stab_ref.3) | copy-start | bytes 100
  37.6 18.0 %copy-start.7 = (bf16[1024,512]{1,0:T(8,128)(2,1)S(1)}, bf16[1024,512]{1,0:T(8,128)(2,1)}, u32[]{:S(2)}) copy-start(bf16[1024,512]{1,0:T(8,128)(2,1)} %w_ref.3) | copy-start | bytes 3145732
  55.8 5.0 %collective-permute-start.6 = (bf16[4,512]{1,0:T(4,128)(2,1)S(1)}, bf16[4,512]{1,0:T(4,128)(2,1)S(1)}, u32[]{:S(2)}, u32[]{:S(2)}) collective-permute-start(bf16[4,512]{1,0:T(4,128)(2,1)S(1)} %get-tuple-element.63), channel_id=1, source_target_pairs={{0,8},{8,0},{16,24},{24,16},{1,9},{9,1},{17,25},{25,17},{2,10},{10... | collective-permute-start | bytes 12296 | tf_op jit(solution)/shard_map/ppermute | solution.py:28
  57.4 3.6 %collective-permute-start.7 = (bf16[4,512]{1,0:T(4,128)(2,1)S(1)}, bf16[4,512]{1,0:T(4,128)(2,1)S(1)}, u32[]{:S(2)}, u32[]{:S(2)}) collective-permute-start(bf16[4,512]{1,0:T(4,128)(2,1)S(1)} %get-tuple-element.64), channel_id=1, source_target_pairs={{0,16},{8,24},{16,0},{24,8},{1,17},{9,25},{17,1},{25,9},{2,18},{10... | collective-permute-start | bytes 12296 | tf_op jit(solution)/shard_map/ppermute | solution.py:28
  57.9 4.5 %collective-permute-start.8 = (bf16[4,512]{1,0:T(4,128)(2,1)S(1)}, bf16[4,512]{1,0:T(4,128)(2,1)S(1)}, u32[]{:S(2)}, u32[]{:S(2)}) collective-permute-start(bf16[4,512]{1,0:T(4,128)(2,1)S(1)} %get-tuple-element.65), channel_id=1, source_target_pairs={{0,24},{8,16},{16,8},{24,0},{1,25},{9,17},{17,9},{25,1},{2,26},{10... | collective-permute-start | bytes 12296 | tf_op jit(solution)/shard_map/ppermute | solution.py:28
